TPU v7x, 32 devices: a whole 2x2x4 slice. The times are simulated.
32 devices in a mesh: rep: 2 (over x), fs: 8 (over z, y), tp: 2 (over core).
Axes of the slice: x: 2, y: 2, z: 4, core: 2. Of those that a mesh axis runs over, the one named last changes fastest.
Arguments:
- incoming_features: bfloat16 [3072, 2048], P(('rep', 'fs'), 'tp'), may hold values from -6 to 6
- attend_prenormal_scale: bfloat16 [2048], replicated, may hold values from 0.099609375 to 1.8984375
- probe_matrix: bfloat16 [2048, 512], P('fs', 'tp'), may hold values from -0.125 to 0.125
- lookup_matrix: bfloat16 [2048, 512], P('fs', 'tp'), may hold values from -0.125 to 0.125
- content_matrix: bfloat16 [2048, 1024], P('fs', 'tp'), may hold values from -0.125 to 0.125
- forgetting_matrix: bfloat16 [2048, 512], P('fs', 'tp'), may hold values from -0.125 to 0.125
- result_switch_matrix: bfloat16 [2048, 1024], P('fs', 'tp'), may hold values from -0.125 to 0.125
- forgetting_shift: float32 [512], P('tp'), may hold values from -0.5 to 5.5
- spike_forget_logarithm: float32 [3072, 512], P(('rep', 'fs'), 'tp'), may hold values from -0.7 to 0
- attend_unit_scale: bfloat16 [1024], P('tp'), may hold values from 0.099609375 to 1.8984375
- attend_result_matrix: bfloat16 [1024, 2048], P('tp', 'fs'), may hold values from -0.1875 to 0.1875
- perceptron_scale: bfloat16 [2048], replicated, may hold values from 0.099609375 to 1.8984375
- content_expand_matrix: bfloat16 [2048, 4096], P('fs', 'tp'), may hold values from -0.125 to 0.125
- switch_expand_matrix: bfloat16 [2048, 4096], P('fs', 'tp'), may hold values from -0.125 to 0.125
- content_kernel: bfloat16 [3, 4096], P(None, 'tp'), may hold values from -3.5 to 3.5
- switch_kernel: bfloat16 [3, 4096], P(None, 'tp'), may hold values from -3.5 to 3.5
- contract_matrix: bfloat16 [4096, 2048], P('tp', 'fs'), may hold values from -0.09375 to 0.09375
Outputs:
- out_rows: bfloat16 [3072, 2048], P(('rep', 'fs'), 'tp')
All inputs are finite; a program needn't handle non-finite values.
Results may differ from a plain program's by a relative error of at most 0.02.
Values may be sent and summed in bfloat16 or wider, within the bound.
A program may use at most 64 MiB of HBM per device.

v0:
```python
import jax
import jax.numpy as jnp
from jax import lax
from jax.sharding import PartitionSpec as P

HEAD_K = 32
HEAD_V = 64
BLOCK = 64


norm_eps = 1e-06
switch_multiplier = 16.0


def row_norm(content_tokens, gain):
    content_tokens = content_tokens.astype(jnp.float32)
    scaled = content_tokens * lax.rsqrt(
        jnp.mean(content_tokens * content_tokens, axis=-1, keepdims=True) + norm_eps
    )
    return (scaled * gain.astype(jnp.float32)).astype(jnp.bfloat16)


def gated_scan(probe_tokens, lookup_tokens, content_tokens, forgetting_scores):
    length, heads, key_size = probe_tokens.shape
    value_size = content_tokens.shape[-1]
    blocks = length // BLOCK

    def split_blocks(array):
        return array.reshape(blocks, BLOCK, heads, array.shape[-1])

    causal = jnp.arange(BLOCK)[:, None] >= jnp.arange(BLOCK)[None, :]
    highest = lax.Precision.HIGHEST

    def step(state, incoming_tokens):
        query_block, key_block, value_block, decay_block = incoming_tokens
        cumulative = jnp.cumsum(decay_block, axis=0)
        differ = cumulative[:, None] - cumulative[None, :]
        weight = jnp.exp(jnp.where(causal[:, :, None, None], differ, -jnp.inf))
        scores = jnp.einsum("thd,shd,tshd->tsh", query_block, key_block, weight, precision=highest)
        inner = jnp.einsum("tsh,shv->thv", scores, value_block, precision=highest)
        carried = jnp.einsum(
            "thd,hdv->thv", query_block * jnp.exp(cumulative), state, precision=highest
        )
        final = cumulative[-1]
        state = jnp.exp(final)[:, :, None] * state + jnp.einsum(
            "shd,shv->hdv",
            key_block * jnp.exp(final[None] - cumulative),
            value_block,
            precision=highest,
        )
        return (state, inner + carried)

    start_state = jnp.zeros((heads, key_size, value_size), jnp.float32)
    _, result_tokens = lax.scan(
        step,
        start_state,
        (
            split_blocks(probe_tokens),
            split_blocks(lookup_tokens),
            split_blocks(content_tokens),
            split_blocks(forgetting_scores),
        ),
    )
    return result_tokens.reshape(length, heads, value_size)


def attend_unit_results(
    probe_tokens,
    lookup_tokens,
    content_tokens,
    result_switch,
    forgetting_raw,
    spike_forgetting,
    attend_unit_scale,
):
    length = probe_tokens.shape[0]
    heads = probe_tokens.shape[1] // HEAD_K
    forgetting_scores = jax.nn.log_sigmoid(forgetting_raw) / switch_multiplier + spike_forgetting

    def split_heads(array, width):
        return array.astype(jnp.float32).reshape(length, heads, width)

    result_tokens = gated_scan(
        split_heads(probe_tokens, HEAD_K) * HEAD_K ** (-0.5),
        split_heads(lookup_tokens, HEAD_K),
        split_heads(content_tokens, HEAD_V),
        split_heads(forgetting_scores, HEAD_K),
    )
    result_tokens = result_tokens * lax.rsqrt(
        jnp.mean(result_tokens * result_tokens, axis=-1, keepdims=True) + norm_eps
    )
    result_tokens = result_tokens * attend_unit_scale.astype(jnp.float32).reshape(heads, HEAD_V)
    switched_result = result_tokens.reshape(length, heads * HEAD_V) * jax.nn.silu(
        result_switch.astype(jnp.float32)
    )
    return switched_result.astype(jnp.bfloat16)


def causal_conv(content_tokens, taps):
    content_tokens = content_tokens.astype(jnp.float32)
    taps = taps.astype(jnp.float32)
    width = taps.shape[0]
    padded = jnp.pad(content_tokens, ((width - 1, 0), (0, 0)))
    total = jnp.zeros_like(content_tokens)
    for offset in range(width):
        total = total + padded[offset : offset + content_tokens.shape[0]] * taps[offset]
    return total


def shards(
    incoming_features,
    attend_prenormal_scale,
    probe_matrix,
    lookup_matrix,
    content_matrix,
    forgetting_matrix,
    result_switch_matrix,
    forgetting_shift,
    spike_forget_logarithm,
    attend_unit_scale,
    attend_result_matrix,
    perceptron_scale,
    content_expand_matrix,
    switch_expand_matrix,
    content_kernel,
    switch_kernel,
    contract_matrix,
):
    whole_in = lax.all_gather(incoming_features, "tp", axis=1, tiled=True)
    normed = row_norm(whole_in, attend_prenormal_scale)
    pieces = (
        lax.all_gather(probe_matrix, "fs", axis=0, tiled=True),
        lax.all_gather(lookup_matrix, "fs", axis=0, tiled=True),
        lax.all_gather(content_matrix, "fs", axis=0, tiled=True),
        lax.all_gather(forgetting_matrix, "fs", axis=0, tiled=True),
        lax.all_gather(result_switch_matrix, "fs", axis=0, tiled=True),
    )
    columns = normed
    query_sum, key_sum, value_sum, decay_sum, gate_sum = tuple(
        (jnp.dot(columns, piece, preferred_element_type=jnp.float32) for piece in pieces)
    )
    switched_result = attend_unit_results(
        query_sum.astype(jnp.bfloat16),
        key_sum.astype(jnp.bfloat16),
        value_sum.astype(jnp.bfloat16),
        gate_sum.astype(jnp.bfloat16),
        decay_sum + forgetting_shift,
        spike_forget_logarithm,
        attend_unit_scale,
    )
    mixer_partial = jnp.dot(
        switched_result,
        lax.all_gather(attend_result_matrix, "fs", axis=1, tiled=True),
        preferred_element_type=jnp.float32,
    )
    mix = lax.psum_scatter(
        mixer_partial.astype(jnp.bfloat16), "tp", scatter_dimension=1, tiled=True
    )
    middle = (
        incoming_features.astype(jnp.float32) + lax.optimization_barrier(mix).astype(jnp.float32)
    ).astype(jnp.bfloat16)
    whole_mid = lax.all_gather(middle, "tp", axis=1, tiled=True)
    normed_mid = row_norm(whole_mid, perceptron_scale)
    pieces = (
        lax.all_gather(content_expand_matrix, "fs", axis=0, tiled=True),
        lax.all_gather(switch_expand_matrix, "fs", axis=0, tiled=True),
    )
    columns = normed_mid
    value_total = jnp.dot(columns, pieces[0], preferred_element_type=jnp.float32)
    gate_total = jnp.dot(columns, pieces[1], preferred_element_type=jnp.float32)
    conv_value = causal_conv(value_total.astype(jnp.bfloat16), content_kernel)
    conv_gated = causal_conv(gate_total.astype(jnp.bfloat16), switch_kernel)
    hidden = (conv_value * jax.nn.gelu(conv_gated, approximate=True)).astype(jnp.bfloat16)
    down_partial = jnp.dot(
        hidden,
        lax.all_gather(contract_matrix, "fs", axis=1, tiled=True),
        preferred_element_type=jnp.float32,
    )
    ffn = lax.psum_scatter(down_partial.astype(jnp.bfloat16), "tp", scatter_dimension=1, tiled=True)
    return (middle.astype(jnp.float32) + lax.optimization_barrier(ffn).astype(jnp.float32)).astype(
        jnp.bfloat16
    )


def solution(mesh):
    placed = (
        P(("rep", "fs"), "tp"),
        P(),
        P("fs", "tp"),
        P("fs", "tp"),
        P("fs", "tp"),
        P("fs", "tp"),
        P("fs", "tp"),
        P("tp"),
        P(("rep", "fs"), "tp"),
        P("tp"),
        P("tp", "fs"),
        P(),
        P("fs", "tp"),
        P("fs", "tp"),
        P(None, "tp"),
        P(None, "tp"),
        P("tp", "fs"),
    )
    return jax.shard_map(
        shards, mesh=mesh, in_specs=placed, out_specs=P(("rep", "fs"), "tp"), check_vma=False
    )
```

profile of v0, /device:TPU:24, one launch (start us, length us, event | category | flops | bytes accessed | tf_op | source)
XLA Modules:
  0.0 696.0 jit_solution(7244822778492802372)
XLA Ops:
  6.6 0.7 all-gather.10.cloned.1.call-update
  7.3 0.7 all-gather.12.cloned.1.call-update
  10.6 2.6 all_gather.33
  13.4 36.0 %all-gather.10.cloned.1.call-done = bf16[2048,256]{1,0:T(8,128)(2,1)} async-done(((bf16[256,256]{1,0:T(8,128)(2,1)}), bf16[2048,256]{1,0:T(8,128)(2,1)}) %all-gather.10.cloned.1.call-update) | async-done | bytes 1048592 | tf_op jit(solution)/shard_map/all_gather | solution.py:135
  49.5 1.7 fusion.65
  51.2 1.1 reshape.64
  52.4 38.2 %all-gather.12.cloned.1.call-done = bf16[2048,256]{1,0:T(8,128)(2,1)} async-done(((bf16[256,256]{1,0:T(8,128)(2,1)}), bf16[2048,256]{1,0:T(8,128)(2,1)}) %all-gather.12.cloned.1.call-update) | async-done | bytes 1048592 | tf_op jit(solution)/shard_map/all_gather | solution.py:133
  90.6 1.6 fusion.47
  92.5 39.3 %all-gather.16.cloned.1.call-done = bf16[2048,256]{1,0:T(8,128)(2,1)} async-done(((bf16[256,256]{1,0:T(8,128)(2,1)}), bf16[2048,256]{1,0:T(8,128)(2,1)}) %all-gather.16.cloned.1.call-update) | async-done | bytes 1048592 | tf_op jit(solution)/shard_map/all_gather | solution.py:132
  131.8 1.6 fusion.46
  133.6 47.8 %all-gather.14.cloned.1.call-done = bf16[2048,512]{1,0:T(8,128)(2,1)} async-done(((bf16[256,512]{1,0:T(8,128)(2,1)}), bf16[2048,512]{1,0:T(8,128)(2,1)}) %all-gather.14.cloned.1.call-update) | async-done | bytes 2097168 | tf_op jit(solution)/shard_map/all_gather | solution.py:134
  181.4 2.2 fusion.43
  183.6 1.1 reshape.60
  184.7 73.7 %while.13 = (s32[]{:T(128)}, f32[8,32,64]{2,1,0:T(8,128)S(1)}, f32[3,64,8,64]{1,3,2,0:T(8,128)}, f32[3,64,8,32]{3,2,1,0:T(8,128)}, f32[3,64,8,32]{3,2,1,0:T(8,12...) while((s32[]{:T(128)}, f32[8,32,64]{2,1,0:T(8,128)S(1)}, ...), condition=%wide.region_3.4_spmd.clone, body=%wide.region_1.3_spmd.clone.sunk | while | flops 56725504 | bytes 20003956 | solution.py:54
  184.7 1.0 fusion.106
  185.9 4.6 select_exponential_fusion.2
  190.5 9.6 %copy.122 = f32[64,64,8,32]{0,1,3,2:T(8,128)} copy(f32[64,64,8,32]{1,3,2,0:T(8,128)} %select_exponential_fusion.2) | data formatting | bytes 8388608 | tf_op jit(solution)/shard_map/while
  200.4 5.3 fusion.108
  205.6 1.0 constant_dynamic-slice_fusion.2
  207.3 1.3 fusion.109
  209.3 1.0 fusion.106
  210.5 4.6 select_exponential_fusion.2
  215.1 9.5 %copy.122 = f32[64,64,8,32]{0,1,3,2:T(8,128)} copy(f32[64,64,8,32]{1,3,2,0:T(8,128)} %select_exponential_fusion.2) | data formatting | bytes 8388608 | tf_op jit(solution)/shard_map/while
  224.9 5.2 fusion.108
  230.2 1.0 constant_dynamic-slice_fusion.2
  231.9 1.3 fusion.109
  233.8 1.0 fusion.106
  235.0 4.6 select_exponential_fusion.2
  239.6 9.6 %copy.122 = f32[64,64,8,32]{0,1,3,2:T(8,128)} copy(f32[64,64,8,32]{1,3,2,0:T(8,128)} %select_exponential_fusion.2) | data formatting | bytes 8388608 | tf_op jit(solution)/shard_map/while
  249.5 5.2 fusion.108
  254.7 1.0 constant_dynamic-slice_fusion.2
  256.4 1.3 fusion.109
  258.4 1.5 copy.86
  260.6 20.8 %all-gather.20.cloned.1.call-done = bf16[512,2048]{1,0:T(8,128)(2,1)} async-done(((bf16[512,256]{1,0:T(8,128)(2,1)}), bf16[512,2048]{1,0:T(8,128)(2,1)}) %all-gather.20.cloned.1.call-update) | async-done | bytes 2097168 | tf_op jit(solution)/shard_map/all_gather | solution.py:153
  281.4 4.4 convolution_convert_fusion.3
  285.9 0.7 all-gather.24.cloned.1.call-update
  286.6 0.7 all-gather.22.cloned.1.call-update
  288.1 6.4 reduce-scatter.3.cloned.1.call-done
  294.4 1.1 add_convert_fusion.1
  295.6 2.5 all_gather.40
  298.3 121.7 %all-gather.24.cloned.1.call-done = bf16[2048,2048]{1,0:T(8,128)(2,1)} async-done(((bf16[256,2048]{1,0:T(8,128)(2,1)}), bf16[2048,2048]{1,0:T(8,128)(2,1)}) %all-gather.24.cloned.1.call-update) | async-done | bytes 8388624 | tf_op jit(solution)/shard_map/all_gather | solution.py:166
  420.0 5.2 fusion.17
  425.3 119.6 %all-gather.22.cloned.1.call-done = bf16[2048,2048]{1,0:T(8,128)(2,1)} async-done(((bf16[256,2048]{1,0:T(8,128)(2,1)}), bf16[2048,2048]{1,0:T(8,128)(2,1)}) %all-gather.22.cloned.1.call-update) | async-done | bytes 8388624 | tf_op jit(solution)/shard_map/all_gather | solution.py:165
  544.8 6.4 fusion.18
  551.2 118.7 %all-gather.26.cloned.1.call-done = bf16[2048,2048]{1,0:T(8,128)(2,1)} async-done(((bf16[2048,256]{1,0:T(8,128)(2,1)}), bf16[2048,2048]{1,0:T(8,128)(2,1)}) %all-gather.26.cloned.1.call-update) | async-done | bytes 8388624 | tf_op jit(solution)/shard_map/all_gather | solution.py:176
  669.9 9.1 %convolution_convert_fusion = bf16[192,2048]{1,0:T(8,128)(2,1)} fusion(bf16[2048,2048]{1,0:T(8,128)(2,1)} %all-gather.26.cloned.1.call-done, f32[192,2048]{1,0:T(8,128)} %fusion.18, f32[192,2048]{1,0:T(8,128)S(1)} %fusion.17, f32[2048]{0:T(1024)S(1)} %bitcast.92, f32[2048]{0:T(1024)S(1)} %bitcast.91, f32[2048]{0:T(1024)S(1)} %bitcast.90, ...), kind=kOutput, calls=%fused_computation.29 | convolution fusion | flops 1618870272 | bytes 12369920 | tf_op jit(solution)/shard_map/dot_general | solution.py:174
  679.0 8.6 %reduce-scatter.5.cloned.1.call-done = bf16[192,1024]{1,0:T(8,128)(2,1)} async-done(((bf16[192,2048]{1,0:T(8,128)(2,1)}), bf16[192,1024]{1,0:T(8,128)(2,1)}) %reduce-scatter.5.cloned.1.call-update) | async-done | bytes 393232 | tf_op jit(solution)/shard_map/reduce_scatter | solution.py:179
  687.6 1.9 add_convert_fusion
  (91 shorter events, 10.1 us)
Async XLA Ops:
  6.5 6.9 copy-start.6
  6.5 6.9 copy-start.8
  6.5 42.9 %copy-start.9 = (f32[192,256]{1,0:T(8,128)S(1)}, f32[192,256]{1,0:T(8,128)}, u32[]{:S(2)}) copy-start(f32[192,256]{1,0:T(8,128)} %param.27) | copy-start | bytes 589828
  6.5 42.9 %copy-start.10 = (f32[256]{0:T(256)S(1)}, f32[256]{0:T(256)}, u32[]{:S(2)}) copy-start(f32[256]{0:T(256)} %param.26) | copy-start | bytes 3076
  6.5 42.9 %all-gather.10.cloned.1.call-start = ((), (), s32[]{:S(2)}) async-start(), calls=%async_computation.2 | async-start | bytes 1179648 | tf_op jit(solution)/shard_map/all_gather | solution.py:135
  7.3 83.3 %all-gather.12.cloned.1.call-start = ((), (), s32[]{:S(2)}) async-start(), calls=%async_computation.3 | async-start | bytes 1179648 | tf_op jit(solution)/shard_map/all_gather | solution.py:133
  8.0 123.7 %all-gather.16.cloned.1.call-start = ((), (), s32[]{:S(2)}) async-start(), calls=%async_computation.5 | async-start | bytes 1179648 | tf_op jit(solution)/shard_map/all_gather | solution.py:132
  8.8 172.6 %all-gather.14.cloned.1.call-start = ((), (), s32[]{:S(2)}) async-start(), calls=%async_computation.4 | async-start | bytes 2359296 | tf_op jit(solution)/shard_map/all_gather | solution.py:134
  9.3 251.3 %all-gather.18.cloned.1.call-start = ((), (), s32[]{:S(2)}) async-start(), calls=%async_computation.6 | async-start | bytes 2359296 | tf_op jit(solution)/shard_map/all_gather | solution.py:136
  9.9 271.5 %all-gather.20.cloned.1.call-start = ((), (), s32[]{:S(2)}) async-start(), calls=%async_computation.7 | async-start | bytes 2359296 | tf_op jit(solution)/shard_map/all_gather | solution.py:153
  10.5 283.9 %reduce-scatter.3.cloned.1.call-start = ((), (), s32[]{:S(2)}) async-start(), calls=%async_computation.8 | async-start | bytes 1179648 | tf_op jit(solution)/shard_map/reduce_scatter | solution.py:156
  13.1 168.3 %copy-start = (bf16[192,2048]{1,0:T(8,128)(2,1)}, bf16[192,2048]{1,0:T(8,128)(2,1)S(1)}, u32[]{:S(2)}) copy-start(bf16[192,2048]{1,0:T(8,128)(2,1)S(1)} %all_gather.33) | copy-start | bytes 2359300
  258.4 1.8 copy-start.2
  259.9 21.5 %copy-start.1 = (bf16[192,2048]{1,0:T(8,128)(2,1)S(1)}, bf16[192,2048]{1,0:T(8,128)(2,1)}, u32[]{:S(2)}) copy-start(bf16[192,2048]{1,0:T(8,128)(2,1)} %copy-done) | copy-start | bytes 2359300
  285.8 2.2 copy-start.7
  285.8 2.2 copy-start.4
  285.8 2.2 copy-start.5
  285.8 8.6 %copy-start.3 = (bf16[192,1024]{1,0:T(8,128)(2,1)S(1)}, bf16[192,1024]{1,0:T(8,128)(2,1)}, u32[]{:S(2)}) copy-start(bf16[192,1024]{1,0:T(8,128)(2,1)} %param.19) | copy-start | bytes 1179652
  285.8 134.2 %all-gather.24.cloned.1.call-start = ((), (), s32[]{:S(2)}) async-start(), calls=%async_computation.10 | async-start | bytes 9437184 | tf_op jit(solution)/shard_map/all_gather | solution.py:166
  286.6 258.3 %all-gather.22.cloned.1.call-start = ((), (), s32[]{:S(2)}) async-start(), calls=%async_computation.9 | async-start | bytes 9437184 | tf_op jit(solution)/shard_map/all_gather | solution.py:165
  287.3 382.6 %all-gather.26.cloned.1.call-start = ((), (), s32[]{:S(2)}) async-start(), calls=%async_computation.11 | async-start | bytes 9437184 | tf_op jit(solution)/shard_map/all_gather | solution.py:176
  287.9 399.7 %reduce-scatter.5.cloned.1.call-start = ((), (), s32[]{:S(2)}) async-start(), calls=%async_computation.12 | async-start | bytes 1179648 | tf_op jit(solution)/shard_map/reduce_scatter | solution.py:179
Sparse Core Ops, SparseCore 0:
  9.5 39.9 all-gather.9
  51.6 38.9 all-gather.11
  92.7 38.9 all-gather.15
  133.8 47.6 all-gather.13
  183.4 47.6 all-gather.17
  232.9 48.4 all-gather.19
  285.9 8.4 reduce-scatter.2
  296.5 123.4 all-gather.23
  422.2 122.6 all-gather.21
  546.7 123.1 all-gather.25
  679.1 8.4 reduce-scatter.4
where the time goes:
time: 699 us; the launch traced here: 696 us
  waiting for transfers between devices  563 us (81%)
  matrix products  39.9 us (6%)
  local copies, waits for them, and re-layouts  37.7 us (5%)
  other arithmetic  36.6 us (5%)
  between operations  13.5 us (2%)
    all_gather x1, waiting for transfers between devices, shards(): lax.all_gather(switch_expand_matrix, 'fs', axis=0, tiled=True)  122 us
    all_gather x1, waiting for transfers between devices, shards(): lax.all_gather(content_expand_matrix, 'fs', axis=0, tiled=True)  120 us
    all_gather x1, waiting for transfers between devices, shards(): lax.all_gather(contract_matrix, 'fs', axis=1, tiled=True)  119 us
    all_gather x1, waiting for transfers between devices, shards(): lax.all_gather(content_matrix, 'fs', axis=0, tiled=True)  47.8 us
    all_gather x1, waiting for transfers between devices, shards(): lax.all_gather(probe_matrix, 'fs', axis=0, tiled=True)  39.3 us
    all_gather x1, waiting for transfers between devices, shards(): lax.all_gather(lookup_matrix, 'fs', axis=0, tiled=True)  38.2 us
    all_gather x1, waiting for transfers between devices, shards(): lax.all_gather(forgetting_matrix, 'fs', axis=0, tiled=True)  36 us
    while x3, local copies, waits for them, and re-layouts  28.7 us
  transfers between devices with their start and end apart: 11, of which 10 were waited for; matrix products, arithmetic and copies ran while one was open for 14% of the time, Pallas kernels for 0%

commit v1 on v0

v1 whole, which is shorter than its diff:
```python
import functools

import jax
import jax.numpy as jnp
from jax import lax
from jax.experimental import pallas as pl
from jax.experimental.pallas import tpu as pltpu
from jax.sharding import PartitionSpec as P

HEAD_K = 32
HEAD_V = 64
SUB = 16

norm_eps = 1e-06
switch_multiplier = 16.0
MESH = pl.DeviceIdType.MESH
F32 = jnp.float32
BF16 = jnp.bfloat16
HIGHEST = lax.Precision.HIGHEST
VMEM_LIMIT = 60 * 1024 * 1024


def row_norm(content_tokens, gain):
    content_tokens = content_tokens.astype(F32)
    scaled = content_tokens * lax.rsqrt(
        jnp.mean(content_tokens * content_tokens, axis=-1, keepdims=True) + norm_eps
    )
    return (scaled * gain.astype(F32)).astype(BF16)


def factor(n):
    inner = 1
    for size in range(1, n + 1):
        if n % size == 0 and size * size <= n:
            inner = size
    return n // inner, inner


def place(ref, axis, index, size):
    at = pl.ds(pl.multiple_of(index * size, size), size)
    return ref.at[at, :] if axis == 0 else ref.at[:, at]


def gather_weights(pieces, axes, group_piece, sizes, collective_id):
    n_rep, n_fs, n_tp = sizes
    outer, inner = factor(n_fs)
    count = len(pieces)
    has_group = group_piece is not None
    group = n_rep * n_tp
    full = []
    for piece, axis in zip(pieces, axes):
        shape = list(piece.shape)
        shape[axis] *= n_fs
        full.append(jax.ShapeDtypeStruct(tuple(shape), piece.dtype))
    ins = list(pieces)
    if has_group:
        ins.append(group_piece)
        full.append(
            jax.ShapeDtypeStruct(
                (group_piece.shape[0] * n_rep, group_piece.shape[1] * n_tp), group_piece.dtype
            )
        )

    def kernel(*refs):
        sources = refs[: len(ins)]
        outs = refs[len(ins) : 2 * len(ins)]
        far_send, far_recv, near_send, near_recv, own_sem, group_send, group_recv = refs[
            2 * len(ins) :
        ]
        rep, fs, tp = lax.axis_index("rep"), lax.axis_index("fs"), lax.axis_index("tp")
        a, b = fs // inner, lax.rem(fs, inner)
        far = [lax.rem(a + d, outer) * inner + b for d in range(1, outer)]
        near = [a * inner + lax.rem(b + d, inner) for d in range(1, inner)]
        barrier = pltpu.get_barrier_semaphore()
        peers = [{"fs": index} for index in far + near]
        others = []
        if has_group:
            for i in range(n_rep):
                for j in range(n_tp):
                    if i or j:
                        others.append(
                            {"rep": lax.rem(rep + i, n_rep), "tp": lax.rem(tp + j, n_tp)}
                        )
        for peer in peers + others:
            pl.semaphore_signal(barrier, inc=1, device_id=peer, device_id_type=MESH)
        pl.semaphore_wait(barrier, len(peers) + len(others))

        waits = []
        if has_group:
            rows, columns = group_piece.shape
            source, out = sources[-1], outs[-1]
            target = out.at[
                pl.ds(pl.multiple_of(rep * rows, rows), rows),
                pl.ds(pl.multiple_of(tp * columns, columns), columns),
            ]
            own = pltpu.make_async_copy(source, target, own_sem.at[count])
            own.start()
            waits.append(own)
            for d, peer in enumerate(others):
                copy = pltpu.make_async_remote_copy(
                    src_ref=source,
                    dst_ref=target,
                    send_sem=group_send.at[d],
                    recv_sem=group_recv.at[d],
                    device_id=peer,
                    device_id_type=MESH,
                )
                copy.start()
                waits.append(copy)
        far_copies = []
        for w in range(count):
            axis, size = axes[w], pieces[w].shape[axes[w]]
            target = place(outs[w], axis, fs, size)
            copies = []
            for d, index in enumerate(far):
                copy = pltpu.make_async_remote_copy(
                    src_ref=sources[w],
                    dst_ref=target,
                    send_sem=far_send.at[w, d],
                    recv_sem=far_recv.at[w, d],
                    device_id={"fs": index},
                    device_id_type=MESH,
                )
                copy.start()
                copies.append(copy)
            far_copies.append(copies)
            for e, index in enumerate(near):
                copy = pltpu.make_async_remote_copy(
                    src_ref=sources[w],
                    dst_ref=target,
                    send_sem=near_send.at[w, 0, e],
                    recv_sem=near_recv.at[w, 0, e],
                    device_id={"fs": index},
                    device_id_type=MESH,
                )
                copy.start()
                waits.append(copy)
            own = pltpu.make_async_copy(sources[w], target, own_sem.at[w])
            own.start()
            waits.append(own)
        for w in range(count):
            axis, size = axes[w], pieces[w].shape[axes[w]]
            for d in range(1, outer):
                far_copies[w][d - 1].wait_recv()
                block = place(outs[w], axis, lax.rem(a + outer - d, outer) * inner + b, size)
                for e, index in enumerate(near):
                    copy = pltpu.make_async_remote_copy(
                        src_ref=block,
                        dst_ref=block,
                        send_sem=near_send.at[w, d, e],
                        recv_sem=near_recv.at[w, d, e],
                        device_id={"fs": index},
                        device_id_type=MESH,
                    )
                    copy.start()
                    waits.append(copy)
        for copies in far_copies:
            for copy in copies:
                copy.wait_send()
        for copy in waits:
            copy.wait()

    dma = pltpu.SemaphoreType.DMA
    return pl.pallas_call(
        kernel,
        out_shape=full,
        in_specs=[pl.BlockSpec(memory_space=pltpu.VMEM)] * len(ins),
        out_specs=[pl.BlockSpec(memory_space=pl.ANY)] * len(ins),
        scratch_shapes=[
            dma((count, max(outer - 1, 1))),
            dma((count, max(outer - 1, 1))),
            dma((count, outer, max(inner - 1, 1))),
            dma((count, outer, max(inner - 1, 1))),
            dma((count + 1,)),
            dma((group,)),
            dma((group,)),
        ],
        compiler_params=pltpu.CompilerParams(
            collective_id=collective_id, has_side_effects=True, vmem_limit_bytes=VMEM_LIMIT
        ),
        name="gather_weights",
    )(*ins)


def reduce_group(partial, base, sizes, spread, collective_id):
    n_rep, n_fs, n_tp = sizes
    rows, columns = base.shape

    def kernel(*refs):
        part_ref, base_ref = refs[:2]
        if spread:
            out_ref, all_ref, slot_a, held, slot_b, send_sem, recv_sem = refs[2:]
        else:
            out_ref, slot_a, held, slot_b, send_sem, recv_sem = refs[2:]
        rep, tp = lax.axis_index("rep"), lax.axis_index("tp")
        tps = [lax.rem(tp + d, n_tp) for d in range(1, n_tp)]
        reps = [lax.rem(rep + d, n_rep) for d in range(1, n_rep)]
        barrier = pltpu.get_barrier_semaphore()
        for index in tps:
            pl.semaphore_signal(barrier, inc=1, device_id={"tp": index}, device_id_type=MESH)
        for index in reps:
            pl.semaphore_signal(barrier, inc=1, device_id={"rep": index}, device_id_type=MESH)
        pl.semaphore_wait(barrier, len(tps) + len(reps))

        def send(stage, d, source, target, peer):
            copy = pltpu.make_async_remote_copy(
                src_ref=source,
                dst_ref=target,
                send_sem=send_sem.at[stage, d],
                recv_sem=recv_sem.at[stage, d],
                device_id=peer,
                device_id_type=MESH,
            )
            copy.start()
            return copy

        copies = [
            send(0, d, place(part_ref, 1, index, columns), slot_a.at[d], {"tp": index})
            for d, index in enumerate(tps)
        ]
        for copy in copies:
            copy.wait()
        total = place(part_ref, 1, tp, columns)[...].astype(F32)
        for d in range(len(tps)):
            total = total + slot_a[d].astype(F32)
        held[...] = total.astype(BF16)
        copies = [
            send(1, d, place(held, 0, index, rows), slot_b.at[d], {"rep": index})
            for d, index in enumerate(reps)
        ]
        for copy in copies:
            copy.wait()
        total = place(held, 0, rep, rows)[...].astype(F32)
        for d in range(len(reps)):
            total = total + slot_b[d].astype(F32)
        result = (base_ref[...].astype(F32) + total.astype(BF16).astype(F32)).astype(BF16)
        out_ref[...] = result
        if spread:
            block = all_ref.at[
                pl.ds(pl.multiple_of(rep * rows, rows), rows),
                pl.ds(pl.multiple_of(tp * columns, columns), columns),
            ]
            block[...] = result
            copies = [send(2, d, block, block, {"rep": index}) for d, index in enumerate(reps)]
            for copy in copies:
                copy.wait()
            strip = place(all_ref, 1, tp, columns)
            copies = [send(3, d, strip, strip, {"tp": index}) for d, index in enumerate(tps)]
            for copy in copies:
                copy.wait()

    out_shape = [jax.ShapeDtypeStruct((rows, columns), BF16)]
    if spread:
        out_shape.append(jax.ShapeDtypeStruct((rows * n_rep, columns * n_tp), BF16))
    vmem = pl.BlockSpec(memory_space=pltpu.VMEM)
    most = max(n_rep, n_tp)
    return pl.pallas_call(
        kernel,
        out_shape=out_shape,
        in_specs=[vmem, vmem],
        out_specs=[vmem] * len(out_shape),
        scratch_shapes=[
            pltpu.VMEM((max(n_tp - 1, 1), rows * n_rep, columns), BF16),
            pltpu.VMEM((rows * n_rep, columns), BF16),
            pltpu.VMEM((max(n_rep - 1, 1), rows, columns), BF16),
            pltpu.SemaphoreType.DMA((4, most)),
            pltpu.SemaphoreType.DMA((4, most)),
        ],
        compiler_params=pltpu.CompilerParams(
            collective_id=collective_id, has_side_effects=True, vmem_limit_bytes=VMEM_LIMIT
        ),
        name="reduce_group",
    )(partial, base)


def lanes_same(shape, row_width, column_width):
    return (
        lax.broadcasted_iota(jnp.int32, shape, 0) // row_width
        == lax.broadcasted_iota(jnp.int32, shape, 1) // column_width
    ).astype(F32)


def dot32(left, right, contract=((1,), (0,))):
    return lax.dot_general(
        left, right, (contract, ((), ())), precision=HIGHEST, preferred_element_type=F32
    )


def attend_kernel(sums_ref, shift_ref, spike_ref, scale_ref, out_ref, *, heads):
    length = sums_ref.shape[0]
    key_lanes, value_lanes = heads * HEAD_K, heads * HEAD_V

    def part(start, width):
        return sums_ref[:, start : start + width]

    def rounded(array):
        return array.astype(BF16).astype(F32)

    query = rounded(part(0, key_lanes)) * HEAD_K ** (-0.5)
    keys = rounded(part(key_lanes, key_lanes))
    values = rounded(part(2 * key_lanes, value_lanes))
    decay_pre = part(2 * key_lanes + value_lanes, key_lanes) + shift_ref[...]
    gate = rounded(part(3 * key_lanes + value_lanes, value_lanes))
    log_sigmoid = jnp.minimum(decay_pre, 0.0) - jnp.log1p(jnp.exp(-jnp.abs(decay_pre)))
    c = log_sigmoid / switch_multiplier + spike_ref[...]
    row = lax.broadcasted_iota(jnp.int32, (length, key_lanes), 0)
    step = 1
    while step < length:
        c = c + jnp.where(row >= step, pltpu.roll(c, step, 0), 0.0)
        step *= 2

    spread = lanes_same((key_lanes, value_lanes), HEAD_K, HEAD_V)
    in_sub = lax.rem(row, SUB)
    out = dot32(query * keys, spread) * values
    for d in range(1, SUB):
        ok = in_sub >= d
        weight = jnp.exp(jnp.where(ok, c - pltpu.roll(c, d, 0), 0.0))
        product = jnp.where(ok, query * pltpu.roll(keys, d, 0) * weight, 0.0)
        out = out + dot32(product, spread) * pltpu.roll(values, d, 0)

    pieces = [jnp.zeros((SUB, value_lanes), F32)]
    stack = heads * SUB
    key_mask = lanes_same((stack, key_lanes), SUB, HEAD_K)
    value_mask = lanes_same((stack, value_lanes), SUB, HEAD_V)
    for start in range(SUB, length, SUB):
        edge = c[start - 1 : start]
        q_part = query[start : start + SUB] * jnp.exp(c[start : start + SUB] - edge)
        k_part = keys[:start] * jnp.exp(edge - c[:start])
        stacked = jnp.concatenate([q_part] * heads, axis=0) * key_mask
        scores = dot32(stacked, k_part, ((1,), (1,)))
        read = dot32(scores, values[:start]) * value_mask
        total = read[:SUB]
        for h in range(1, heads):
            total = total + read[h * SUB : (h + 1) * SUB]
        pieces.append(total)
    out = out + jnp.concatenate(pieces, axis=0)

    same = lanes_same((value_lanes, value_lanes), HEAD_V, HEAD_V)
    mean = dot32(out * out, same) / HEAD_V
    out = out * lax.rsqrt(mean + norm_eps) * scale_ref[...]
    out_ref[...] = (out * (gate / (1.0 + jnp.exp(-gate)))).astype(BF16)


def attend(sums, shift, spike, scale, length):
    heads = shift.shape[0] // HEAD_K
    value_lanes = heads * HEAD_V
    rows = sums.shape[0]
    return pl.pallas_call(
        functools.partial(attend_kernel, heads=heads),
        grid=(rows // length,),
        out_shape=jax.ShapeDtypeStruct((rows, value_lanes), BF16),
        in_specs=[
            pl.BlockSpec((length, sums.shape[1]), lambda i: (i, 0)),
            pl.BlockSpec((1, shift.shape[0]), lambda i: (0, 0)),
            pl.BlockSpec((length, shift.shape[0]), lambda i: (i, 0)),
            pl.BlockSpec((1, value_lanes), lambda i: (0, 0)),
        ],
        out_specs=pl.BlockSpec((length, value_lanes), lambda i: (i, 0)),
        compiler_params=pltpu.CompilerParams(vmem_limit_bytes=VMEM_LIMIT),
        name="attend",
    )(sums, shift.reshape(1, -1), spike, scale.astype(F32).reshape(1, -1))


def causal_conv(content_tokens, taps, length):
    rows, columns = content_tokens.shape
    content_tokens = content_tokens.astype(F32).reshape(rows // length, length, columns)
    taps = taps.astype(F32)
    width = taps.shape[0]
    padded = jnp.pad(content_tokens, ((0, 0), (width - 1, 0), (0, 0)))
    total = jnp.zeros_like(content_tokens)
    for offset in range(width):
        total = total + padded[:, offset : offset + length] * taps[offset]
    return total.reshape(rows, columns)


def shards(
    sizes,
    incoming_features,
    attend_prenormal_scale,
    probe_matrix,
    lookup_matrix,
    content_matrix,
    forgetting_matrix,
    result_switch_matrix,
    forgetting_shift,
    spike_forget_logarithm,
    attend_unit_scale,
    attend_result_matrix,
    perceptron_scale,
    content_expand_matrix,
    switch_expand_matrix,
    content_kernel,
    switch_kernel,
    contract_matrix,
):
    n_rep, n_fs, n_tp = sizes
    rep = lax.axis_index("rep")
    length = incoming_features.shape[0]

    def mine(array, axis):
        size = array.shape[axis] // n_rep
        return lax.dynamic_slice_in_dim(array, rep * size, size, axis)

    project = jnp.concatenate(
        [
            mine(matrix, 1)
            for matrix in (
                probe_matrix,
                lookup_matrix,
                content_matrix,
                forgetting_matrix,
                result_switch_matrix,
            )
        ],
        axis=1,
    )
    project_all, whole_in = gather_weights((project,), (0,), incoming_features, sizes, 0)
    spike_all = lax.all_to_all(
        spike_forget_logarithm, "rep", split_axis=1, concat_axis=0, tiled=True
    )
    normed = row_norm(whole_in, attend_prenormal_scale)
    sums = jnp.dot(normed, project_all, preferred_element_type=F32)
    expand = jnp.concatenate([mine(content_expand_matrix, 1), mine(switch_expand_matrix, 1)], axis=1)
    side = attend_result_matrix.shape[1]
    axis = 1 if side % 128 == 0 else 0
    result_all, expand_all, contract_all = gather_weights(
        (mine(attend_result_matrix, 0), expand, mine(contract_matrix, 0)),
        (axis, 0, axis),
        None,
        sizes,
        1,
    )
    if axis == 0:
        result_all, contract_all = (
            array.reshape(n_fs, -1, side).swapaxes(0, 1).reshape(-1, n_fs * side)
            for array in (result_all, contract_all)
        )
    switched_result = attend(
        sums,
        mine(forgetting_shift, 0),
        spike_all,
        mine(attend_unit_scale, 0),
        length,
    )
    mixer_partial = jnp.dot(switched_result, result_all, preferred_element_type=F32).astype(BF16)
    middle, whole_mid = reduce_group(mixer_partial, incoming_features, sizes, True, 2)
    normed_mid = row_norm(whole_mid, perceptron_scale)
    both = jnp.dot(normed_mid, expand_all, preferred_element_type=F32).astype(BF16)
    half = both.shape[1] // 2
    conv_value = causal_conv(both[:, :half], mine(content_kernel, 1), length)
    conv_gated = causal_conv(both[:, half:], mine(switch_kernel, 1), length)
    hidden = (conv_value * jax.nn.gelu(conv_gated, approximate=True)).astype(BF16)
    down_partial = jnp.dot(hidden, contract_all, preferred_element_type=F32).astype(BF16)
    return reduce_group(down_partial, middle, sizes, False, 3)[0]


def solution(mesh):
    sizes = (mesh.shape["rep"], mesh.shape["fs"], mesh.shape["tp"])
    placed = (
        P(("rep", "fs"), "tp"),
        P(),
        P("fs", "tp"),
        P("fs", "tp"),
        P("fs", "tp"),
        P("fs", "tp"),
        P("fs", "tp"),
        P("tp"),
        P(("rep", "fs"), "tp"),
        P("tp"),
        P("tp", "fs"),
        P(),
        P("fs", "tp"),
        P("fs", "tp"),
        P(None, "tp"),
        P(None, "tp"),
        P("tp", "fs"),
    )
    return jax.shard_map(
        functools.partial(shards, sizes),
        mesh=mesh,
        in_specs=placed,
        out_specs=P(("rep", "fs"), "tp"),
        check_vma=False,
    )
```

time: 699 us -> 374 us (0.54)
  waiting for transfers between devices: 563 us -> 0.01 us
  Pallas kernels: 0 us -> 331 us
  other arithmetic: 36.6 us -> 7.4 us
  local copies, waits for them, and re-layouts: 37.7 us -> 13.7 us
  matrix products: 39.9 us -> 17.5 us
  between operations: 13.5 us -> 0.27 us
    all_gather x9 -> x0, waiting for transfers between devices: 542 us -> none  [the longest x1 122 us: shards(): lax.all_gather(switch_expand_matrix, 'fs', axis=0, tiled=True)]
    pallas_call x0 -> x5, Pallas kernels: none -> 331 us  [the longest x2 271 us: gather_weights(): pl.pallas_call(kernel, out_shape=full, in_specs=[pl.BlockSpec(memory_spac...]
    while x4 -> x0, local copies, waits for them, and re-layouts: 30.2 us -> none
    dot_general x17 -> x4, matrix products: 39.9 us -> 17.5 us  [the longest x1 6.84 us: shards(): jnp.dot(normed_mid, expand_all, preferred_element_type=F32).astype(BF16)]
    dot_general x3 -> x0, other arithmetic: 15.7 us -> none  [step(): jnp.einsum('thd,shd,tshd->tsh', query_block, key_block, weight, precision...]
    reduce_scatter x2 -> x0, waiting for transfers between devices: 15 us -> none  [the longest x1 8.6 us: shards(): lax.psum_scatter(down_partial.astype(jnp.bfloat16), 'tp', scatter_dimensi...]
    exp x3 -> x0, other arithmetic: 13.9 us -> none  [step(): weight = jnp.exp(jnp.where(causal[:, :, None, None], differ, -jnp.inf))]
    unnamed x22 -> x35, local copies, waits for them, and re-layouts: 0.05 us -> 8.66 us
  transfers between devices with their start and end apart: 11 -> 1, of which waited for: 10 -> 0; matrix products, arithmetic and copies ran while one was open for 14% -> 4% of each run, Pallas kernels for 0% -> 73%
where the time goes in v1:
time: 374 us; the launch traced here: 373 us
  Pallas kernels  331 us (89%)
  matrix products  17.5 us (5%)
  local copies, waits for them, and re-layouts  13.7 us (4%)
  other arithmetic  7.4 us (2%)
    pallas_call x2, Pallas kernels, gather_weights(): pl.pallas_call(kernel, out_shape=full, in_specs=[pl.BlockSpec(memory_spac...  271 us
    pallas_call x2, Pallas kernels, reduce_group(): pl.pallas_call(kernel, out_shape=out_shape, in_specs=[vmem, vmem], out_sp...  45.3 us
    pallas_call x1, Pallas kernels, attend(): pl.pallas_call(functools.partial(attend_kernel, heads=heads), grid=(rows...  14.4 us
    unnamed x35, local copies, waits for them, and re-layouts  8.66 us
  transfers between devices with their start and end apart: 1, of which 0 were waited for; matrix products, arithmetic and copies ran while one was open for 4% of the time, Pallas kernels for 73%

profile of v1, /device:TPU:24, one launch (start us, length us, event | category | flops | bytes accessed | tf_op | source)
XLA Modules:
  0.0 373.0 jit_solution(11791084993143666804)
XLA Ops:
  0.0 0.0 copy-start
  0.0 1.7 copy_bitcast_fusion
  1.7 3.4 all-to-all-start
  5.2 0.9 dynamic-slice_dynamic-update-slice_fusion.4
  6.0 0.9 dynamic-slice_dynamic-update-slice_fusion.3
  6.9 0.9 dynamic-slice_dynamic-update-slice_fusion.1
  7.8 0.0 copy-start.10
  7.8 0.0 copy-start.12
  7.8 0.0 copy-start.11
  7.8 0.9 dynamic-slice_dynamic-update-slice_fusion.2
  8.7 1.6 dynamic-slice_dynamic-update-slice_fusion
  10.4 0.8 copy-done.5
  11.2 65.4 %gather_weights.2 = (bf16[2048,896]{1,0:T(8,128)(2,1)}, bf16[384,2048]{1,0:T(8,128)(2,1)}) custom-call(bf16[256,896]{1,0:T(8,128)(2,1)} %copy-done.5, bf16[192,1024]{1,0:T(8,128)(2,1)} %refs_1_.3), custom_call_target="tpu_custom_call" | custom-call | tf_op jit(solution)/shard_map/gather_weights/pallas_call | solution.py:164
  76.6 0.0 copy-start.6
  76.6 0.0 copy-start.7
  76.6 1.9 fusion
  78.6 0.0 copy-done.10
  78.6 0.0 copy-done.12
  78.6 0.7 dynamic-slice_convert_fusion.2
  79.3 0.0 copy-done.11
  79.3 0.0 copy-done
  79.3 0.8 constant_dynamic-slice_fusion.refs_2_
  80.1 0.0 copy-done.9
  80.2 0.1 constant_dynamic-slice_fusion.1
  80.3 1.1 pad_maximum_fusion.refs_1_
  81.4 0.7 copy-done.1
  82.1 5.0 %fusion.24.sums_ref = f32[384,896]{1,0:T(8,128)} fusion(bf16[2048,896]{1,0:T(8,128)(2,1)} %get-tuple-element.13, bf16[384,2048]{1,0:T(8,128)(2,1)S(1)} %copy-done.1, f32[2048]{0:T(1024)S(1)} %convert_element_type.43, f32[384]{0:T(512)S(1)} %add_rsqrt_fusion.1), kind=kOutput, calls=%fused_computation.35 | convolution fusion | flops 1412431872 | bytes 6628864 | tf_op jit(solution)/shard_map/dot_general | solution.py:422
  87.1 205.5 %gather_weights.3 = (bf16[256,2048]{1,0:T(8,128)(2,1)}, bf16[2048,2048]{1,0:T(8,128)(2,1)}, bf16[1024,2048]{1,0:T(8,128)(2,1)}) custom-call(bf16[256,256]{1,0:T(8,128)(2,1)} %get-tuple-element.28.refs_0_, bf16[256,2048]{1,0:T(8,128)(2,1)} %pad_maximum_fusion.refs_1_, bf16[1024,256]{1,0:T(8,128)(2,1)} %constant_dynamic-slice_fusion.refs_2_), custom_call_target="tpu_custom_call" | custom-call | tf_op jit(solution)/shard_map/gather_weights/pallas_call | solution.py:164
  292.6 0.6 dynamic-slice_bitcast_fusion.shift_ref
  293.2 0.0 all-to-all-done
  293.2 0.7 copy-done.4
  293.9 14.4 %attend.1 = bf16[384,256]{1,0:T(8,128)(2,1)} custom-call(f32[384,896]{1,0:T(8,128)} %fusion.24.sums_ref, f32[1,128]{1,0:T(1,128)} %dynamic-slice_bitcast_fusion.shift_ref, f32[384,128]{1,0:T(8,128)} %bitcast.33, f32[1,256]{1,0:T(1,128)} %bitcast.40), custom_call_target="tpu_custom_call" | custom-call | tf_op jit(solution)/shard_map/attend/pallas_call | solution.py:348
  308.3 2.7 convolution_convert_fusion.2.refs_0_
  311.0 29.0 %reduce_group.2 = (bf16[192,1024]{1,0:T(8,128)(2,1)}, bf16[384,2048]{1,0:T(8,128)(2,1)}) custom-call(bf16[384,2048]{1,0:T(8,128)(2,1)} %convolution_convert_fusion.2.refs_0_, bf16[192,1024]{1,0:T(8,128)(2,1)} %refs_1_.3), custom_call_target="tpu_custom_call" | custom-call | tf_op jit(solution)/shard_map/reduce_group/pallas_call | solution.py:257
  339.9 0.0 copy-start.2
  340.0 1.9 fusion.3
  341.9 0.0 copy-done.2
  341.9 6.8 %convolution_convert_fusion = bf16[384,2048]{1,0:T(8,128)(2,1)S(1)} fusion(bf16[2048,2048]{1,0:T(8,128)(2,1)} %get-tuple-element.16, bf16[384,2048]{1,0:T(8,128)(2,1)S(1)} %copy-done.2, f32[2048]{0:T(1024)S(1)} %convert_element_type.47, f32[384]{0:T(512)S(1)} %add_rsqrt_fusion), kind=kOutput, calls=%fused_computation.10 | convolution fusion | flops 3225157632 | bytes 11544064 | tf_op jit(solution)/shard_map/dot_general | solution.py:448
  348.7 0.1 fusion.30
  348.9 0.2 convert.3
  349.0 0.2 convert.4
  349.2 0.5 fusion.8
  349.7 0.5 fusion.12
  350.2 0.5 fusion.22
  350.7 1.2 copy-done.13
  351.9 3.0 convolution_convert_fusion.1.refs_0_
  354.9 16.3 %reduce_group.3 = bf16[192,1024]{1,0:T(8,128)(2,1)} custom-call(bf16[384,2048]{1,0:T(8,128)(2,1)} %convolution_convert_fusion.1.refs_0_, bf16[192,1024]{1,0:T(8,128)(2,1)} %get-tuple-element.18.refs_1_), custom_call_target="tpu_custom_call" | custom-call | tf_op jit(solution)/shard_map/reduce_group/pallas_call | solution.py:257
  371.2 1.8 copy.26
  (20 shorter events, 0.1 us)
Async XLA Ops:
  0.0 79.3 %copy-start = (bf16[2048,256]{1,0:T(8,128)(2,1)S(1)}, bf16[2048,256]{1,0:T(8,128)(2,1)}, u32[]{:S(2)}) copy-start(bf16[2048,256]{1,0:T(8,128)(2,1)} %param.33) | copy-start | bytes 3145732
  1.7 291.5 %all-to-all-start = ((f32[192,2,128]{2,0,1:T(8,128)}), f32[192,2,128]{2,0,1:T(8,128)S(1)}, u32[]{:S(2)}, u32[]{:S(2)}) async-start(f32[192,2,128]{2,0,1:T(8,128)} %copy_bitcast_fusion), calls=%async_computation | async-start | bytes 393216 | tf_op jit(solution)/shard_map/all_to_all | solution.py:418
  7.8 70.8 %copy-start.10 = (bf16[2048]{0:T(1024)(128)(2,1)S(1)}, bf16[2048]{0:T(1024)(128)(2,1)}, u32[]{:S(2)}) copy-start(bf16[2048]{0:T(1024)(128)(2,1)} %param.18) | copy-start | bytes 12292
  7.8 70.8 %copy-start.12 = (bf16[512]{0:T(512)(128)(2,1)S(1)}, bf16[512]{0:T(512)(128)(2,1)}, u32[]{:S(2)}) copy-start(bf16[512]{0:T(512)(128)(2,1)} %param.26) | copy-start | bytes 3076
  7.8 71.4 %copy-start.11 = (bf16[2048]{0:T(1024)(128)(2,1)S(1)}, bf16[2048]{0:T(1024)(128)(2,1)}, u32[]{:S(2)}) copy-start(bf16[2048]{0:T(1024)(128)(2,1)} %param.28) | copy-start | bytes 12292
  10.4 0.8 copy-start.5
  11.1 69.0 %copy-start.8 = (bf16[3,2048]{1,0:T(4,128)(2,1)S(1)}, bf16[3,2048]{1,0:T(4,128)(2,1)}, u32[]{:S(2)}) copy-start(bf16[3,2048]{1,0:T(4,128)(2,1)} %param.32) | copy-start | bytes 36868
  11.1 69.0 %copy-start.9 = (bf16[3,2048]{1,0:T(4,128)(2,1)S(1)}, bf16[3,2048]{1,0:T(4,128)(2,1)}, u32[]{:S(2)}) copy-start(bf16[3,2048]{1,0:T(4,128)(2,1)} %param.31) | copy-start | bytes 36868
  76.6 3.6 copy-start.6
  76.6 3.6 copy-start.7
  80.3 1.8 copy-start.1
  87.1 205.5 %copy-start.14 = (f32[256]{0:T(256)S(1)}, f32[256]{0:T(256)}, u32[]{:S(2)}) copy-start(f32[256]{0:T(256)} %param.24) | copy-start | bytes 3076
  292.6 15.7 %copy-start.3 = (bf16[256,2048]{1,0:T(8,128)(2,1)S(1)}, bf16[256,2048]{1,0:T(8,128)(2,1)}, u32[]{:S(2)}) copy-start(bf16[256,2048]{1,0:T(8,128)(2,1)} %get-tuple-element.14) | copy-start | bytes 3145732
  293.2 0.7 copy-start.4
  339.9 1.9 copy-start.2
  349.7 2.2 copy-start.13

commit v2 on v1

v2 whole, which is shorter than its diff:
```python
import functools

import jax
import jax.numpy as jnp
from jax import lax
from jax.experimental import pallas as pl
from jax.experimental.pallas import tpu as pltpu
from jax.sharding import PartitionSpec as P

HEAD_K = 32
HEAD_V = 64
SUB = 16

norm_eps = 1e-06
switch_multiplier = 16.0
MESH = pl.DeviceIdType.MESH
F32 = jnp.float32
BF16 = jnp.bfloat16
HIGHEST = lax.Precision.HIGHEST
VMEM_LIMIT = 60 * 1024 * 1024


def row_norm(content_tokens, gain):
    content_tokens = content_tokens.astype(F32)
    scaled = content_tokens * lax.rsqrt(
        jnp.mean(content_tokens * content_tokens, axis=-1, keepdims=True) + norm_eps
    )
    return (scaled * gain.astype(F32)).astype(BF16)


def factor(n):
    inner = 1
    for size in range(1, n + 1):
        if n % size == 0 and size * size <= n:
            inner = size
    return n // inner, inner


def place(ref, axis, index, size):
    at = pl.ds(pl.multiple_of(index * size, size), size)
    return ref.at[at, :] if axis == 0 else ref.at[:, at]


def send_to(source, target, send_sem, recv_sem, peer):
    copy = pltpu.make_async_remote_copy(
        src_ref=source,
        dst_ref=target,
        send_sem=send_sem,
        recv_sem=recv_sem,
        device_id=peer,
        device_id_type=MESH,
    )
    copy.start()
    return copy


def pieces_of(rows, most):
    for count in range(most, 1, -1):
        if rows % (16 * count) == 0:
            return count
    return 1


def first_half(
    project, result, expand, contract, features, gain, shift, spike, scale, axis, inside, sizes
):
    n_rep, n_fs, n_tp = sizes
    outer, inner = factor(n_fs)
    length, columns = features.shape
    rows = length * n_rep
    heads = shift.shape[0] // HEAD_K
    value_lanes = heads * HEAD_V
    group = n_rep * n_tp
    most = max(n_rep, n_tp)
    weights = (project, result, expand, contract)
    axes = (0, axis, 0, axis)
    splits = (2, 1, 4, 4)
    full = []
    chunks = []
    for w in range(4):
        shape = list(weights[w].shape)
        size = shape[0]
        shape[axes[w]] *= n_fs
        full.append(tuple(shape))
        split = pieces_of(size, splits[w])
        chunks += [(w, k * (size // split), size // split) for k in range(split)]
    count = len(chunks)

    def kernel(*refs):
        sources = refs[:4]
        features_ref, gain_ref, shift_ref, spike_ref, scale_ref = refs[4:9]
        if inside:
            expand_out, contract_out, middle_ref, mid_ref = refs[9:13]
            rest = refs[13:]
            result_out, gated_ref, partial_ref, slot_a, held, slot_b = rest[:6]
            rest = rest[6:]
        else:
            expand_out, contract_out, result_out, gated_ref = refs[9:13]
            rest = refs[13:]
        project_out, whole_ref = rest[:2]
        far_send, far_recv, near_send, near_recv, own_sem, group_send, group_recv = rest[2:9]
        if inside:
            sum_send, sum_recv = rest[9:]
        outs = (project_out, result_out, expand_out, contract_out)
        rep, fs, tp = lax.axis_index("rep"), lax.axis_index("fs"), lax.axis_index("tp")
        a, b = fs // inner, lax.rem(fs, inner)
        far = [lax.rem(a + d, outer) * inner + b for d in range(1, outer)]
        near = [a * inner + lax.rem(b + d, inner) for d in range(1, inner)]
        peers = [{"fs": index} for index in far + near]
        others = [
            {"rep": lax.rem(rep + i, n_rep), "tp": lax.rem(tp + j, n_tp)}
            for i in range(n_rep)
            for j in range(n_tp)
            if i or j
        ]
        barrier = pltpu.get_barrier_semaphore()
        for peer in peers + others:
            pl.semaphore_signal(barrier, inc=1, device_id=peer, device_id_type=MESH)
        pl.semaphore_wait(barrier, len(peers) + len(others))

        def block(w, start, size, index):
            across = weights[w].shape[axes[w]]
            offset = pl.multiple_of(index * across, across)
            if axes[w] == 0:
                return outs[w].at[pl.ds(offset + start, size), :]
            return outs[w].at[pl.ds(start, size), pl.ds(offset, across)]

        far_copies, near_copies, own_copies = {}, {}, {}

        def launch_far(c):
            w, start, size = chunks[c]
            source, target = sources[w].at[pl.ds(start, size), :], block(w, start, size, fs)
            far_copies[c] = [
                send_to(source, target, far_send.at[c, d], far_recv.at[c, d], {"fs": index})
                for d, index in enumerate(far)
            ]

        def launch_near(c):
            w, start, size = chunks[c]
            source, target = sources[w].at[pl.ds(start, size), :], block(w, start, size, fs)
            near_copies[c] = [
                send_to(
                    source, target, near_send.at[c, 0, e], near_recv.at[c, 0, e], {"fs": index}
                )
                for e, index in enumerate(near)
            ]
            own_copies[c] = pltpu.make_async_copy(source, target, own_sem.at[c])
            own_copies[c].start()

        def forward(c):
            w, start, size = chunks[c]
            for d in range(1, outer):
                far_copies[c][d - 1].wait_recv()
                held_block = block(w, start, size, lax.rem(a + outer - d, outer) * inner + b)
                near_copies[c] += [
                    send_to(
                        held_block,
                        held_block,
                        near_send.at[c, d, e],
                        near_recv.at[c, d, e],
                        {"fs": index},
                    )
                    for e, index in enumerate(near)
                ]

        def arrived(c):
            for copy in near_copies[c]:
                copy.wait_recv()
            own_copies[c].wait()

        first = [c for c in range(count) if chunks[c][0] == 0]
        second = [c for c in range(count) if chunks[c][0] == 1]
        later = [c for c in range(count) if chunks[c][0] > 1]

        spot = whole_ref.at[
            pl.ds(pl.multiple_of(rep * length, length), length),
            pl.ds(pl.multiple_of(tp * columns, columns), columns),
        ]
        own = pltpu.make_async_copy(features_ref, spot, own_sem.at[count])
        own.start()
        group_copies = [
            send_to(features_ref, spot, group_send.at[d], group_recv.at[d], peer)
            for d, peer in enumerate(others)
        ]
        for c in first:
            launch_far(c)
            launch_near(c)
        for c in second + later:
            launch_far(c)
        for c in first:
            forward(c)
        for c in second + later:
            launch_near(c)
        for c in first:
            arrived(c)
        own.wait()
        for copy in group_copies:
            copy.wait()

        def sequence(i, carry):
            at = pl.ds(pl.multiple_of(i * length, length), length)
            normed = row_norm(whole_ref[at, :], gain_ref[...])
            sums = jnp.dot(normed, project_out[...], preferred_element_type=F32)
            gated_ref[at, :] = attend_rows(
                sums, shift_ref[...], spike_ref[at, :], scale_ref[...], heads
            )
            return carry

        lax.fori_loop(0, n_rep, sequence, 0)
        for c in second:
            forward(c)
        waiting = list(later)
        for c in waiting[:1]:
            forward(c)
        waiting = waiting[1:]
        for c in second:
            arrived(c)
        if inside:

            def mixer(i, carry):
                at = pl.ds(pl.multiple_of(i * length, length), length)
                partial_ref[at, :] = jnp.dot(
                    gated_ref[at, :], result_out[...], preferred_element_type=F32
                ).astype(BF16)
                return carry

            lax.fori_loop(0, n_rep, mixer, 0)

            def between(stage):
                if stage in (1, 2):
                    forward(waiting.pop(0))

            reduce_steps(
                partial_ref,
                features_ref,
                middle_ref,
                mid_ref,
                slot_a,
                held,
                slot_b,
                sum_send,
                sum_recv,
                sizes,
                between,
            )
        for c in waiting:
            forward(c)
        for c in later:
            arrived(c)
        for c in range(count):
            for copy in far_copies[c] + near_copies[c]:
                copy.wait_send()

    dma = pltpu.SemaphoreType.DMA
    vmem = pl.BlockSpec(memory_space=pltpu.VMEM)
    hbm = pl.BlockSpec(memory_space=pl.ANY)
    out_shape = [jax.ShapeDtypeStruct(full[2], BF16), jax.ShapeDtypeStruct(full[3], BF16)]
    scratch = []
    gated_shape = (rows, value_lanes)
    if inside:
        out_shape += [
            jax.ShapeDtypeStruct((length, columns), BF16),
            jax.ShapeDtypeStruct((rows, columns * n_tp), BF16),
        ]
        out_specs = [hbm, hbm, vmem, vmem]
        scratch += [
            pltpu.VMEM(full[1], BF16),
            pltpu.VMEM(gated_shape, BF16),
            pltpu.VMEM((rows, columns * n_tp), BF16),
            pltpu.VMEM((max(n_tp - 1, 1), rows, columns), BF16),
            pltpu.VMEM((rows, columns), BF16),
            pltpu.VMEM((max(n_rep - 1, 1), length, columns), BF16),
        ]
    else:
        out_shape += [
            jax.ShapeDtypeStruct(full[1], BF16),
            jax.ShapeDtypeStruct(gated_shape, BF16),
        ]
        out_specs = [hbm, hbm, hbm, vmem]
    scratch += [
        pltpu.VMEM(full[0], BF16),
        pltpu.VMEM((rows, columns * n_tp), BF16),
        dma((count, max(outer - 1, 1))),
        dma((count, max(outer - 1, 1))),
        dma((count, outer, max(inner - 1, 1))),
        dma((count, outer, max(inner - 1, 1))),
        dma((count + 1,)),
        dma((group,)),
        dma((group,)),
    ]
    if inside:
        scratch += [dma((4, most)), dma((4, most))]
    return pl.pallas_call(
        kernel,
        out_shape=out_shape,
        in_specs=[vmem] * 9,
        out_specs=out_specs,
        scratch_shapes=scratch,
        compiler_params=pltpu.CompilerParams(
            collective_id=0, has_side_effects=True, vmem_limit_bytes=VMEM_LIMIT
        ),
        name="first_half",
    )(
        *weights,
        features,
        gain.reshape(1, -1),
        shift.reshape(1, -1),
        spike,
        scale.astype(F32).reshape(1, -1),
    )


def reduce_steps(
    part_ref, base_ref, out_ref, all_ref, slot_a, held, slot_b, send_sem, recv_sem, sizes, between
):
    n_rep, n_fs, n_tp = sizes
    rows, columns = base_ref.shape
    rep, tp = lax.axis_index("rep"), lax.axis_index("tp")
    tps = [lax.rem(tp + d, n_tp) for d in range(1, n_tp)]
    reps = [lax.rem(rep + d, n_rep) for d in range(1, n_rep)]

    def send(stage, d, source, target, peer):
        return send_to(source, target, send_sem.at[stage, d], recv_sem.at[stage, d], peer)

    copies = [
        send(0, d, place(part_ref, 1, index, columns), slot_a.at[d], {"tp": index})
        for d, index in enumerate(tps)
    ]
    for copy in copies:
        copy.wait()
    total = place(part_ref, 1, tp, columns)[...].astype(F32)
    for d in range(len(tps)):
        total = total + slot_a[d].astype(F32)
    held[...] = total.astype(BF16)
    copies = [
        send(1, d, place(held, 0, index, rows), slot_b.at[d], {"rep": index})
        for d, index in enumerate(reps)
    ]
    between(1)
    for copy in copies:
        copy.wait()
    total = place(held, 0, rep, rows)[...].astype(F32)
    for d in range(len(reps)):
        total = total + slot_b[d].astype(F32)
    result = (base_ref[...].astype(F32) + total.astype(BF16).astype(F32)).astype(BF16)
    out_ref[...] = result
    if all_ref is not None:
        block = all_ref.at[
            pl.ds(pl.multiple_of(rep * rows, rows), rows),
            pl.ds(pl.multiple_of(tp * columns, columns), columns),
        ]
        block[...] = result
        copies = [send(2, d, block, block, {"rep": index}) for d, index in enumerate(reps)]
        between(2)
        for copy in copies:
            copy.wait()
        strip = place(all_ref, 1, tp, columns)
        copies = [send(3, d, strip, strip, {"tp": index}) for d, index in enumerate(tps)]
        for copy in copies:
            copy.wait()


def reduce_group(partial, base, sizes, spread, collective_id):
    n_rep, n_fs, n_tp = sizes
    rows, columns = base.shape

    def kernel(*refs):
        part_ref, base_ref = refs[:2]
        if spread:
            out_ref, all_ref, slot_a, held, slot_b, send_sem, recv_sem = refs[2:]
        else:
            all_ref = None
            out_ref, slot_a, held, slot_b, send_sem, recv_sem = refs[2:]
        rep, tp = lax.axis_index("rep"), lax.axis_index("tp")
        barrier = pltpu.get_barrier_semaphore()
        for d in range(1, n_tp):
            peer = {"tp": lax.rem(tp + d, n_tp)}
            pl.semaphore_signal(barrier, inc=1, device_id=peer, device_id_type=MESH)
        for d in range(1, n_rep):
            peer = {"rep": lax.rem(rep + d, n_rep)}
            pl.semaphore_signal(barrier, inc=1, device_id=peer, device_id_type=MESH)
        pl.semaphore_wait(barrier, n_tp + n_rep - 2)
        reduce_steps(
            part_ref,
            base_ref,
            out_ref,
            all_ref,
            slot_a,
            held,
            slot_b,
            send_sem,
            recv_sem,
            sizes,
            lambda stage: None,
        )

    out_shape = [jax.ShapeDtypeStruct((rows, columns), BF16)]
    if spread:
        out_shape.append(jax.ShapeDtypeStruct((rows * n_rep, columns * n_tp), BF16))
    vmem = pl.BlockSpec(memory_space=pltpu.VMEM)
    most = max(n_rep, n_tp)
    return pl.pallas_call(
        kernel,
        out_shape=out_shape,
        in_specs=[vmem, vmem],
        out_specs=[vmem] * len(out_shape),
        scratch_shapes=[
            pltpu.VMEM((max(n_tp - 1, 1), rows * n_rep, columns), BF16),
            pltpu.VMEM((rows * n_rep, columns), BF16),
            pltpu.VMEM((max(n_rep - 1, 1), rows, columns), BF16),
            pltpu.SemaphoreType.DMA((4, most)),
            pltpu.SemaphoreType.DMA((4, most)),
        ],
        compiler_params=pltpu.CompilerParams(
            collective_id=collective_id, has_side_effects=True, vmem_limit_bytes=VMEM_LIMIT
        ),
        name="reduce_group",
    )(partial, base)


def lanes_same(shape, row_width, column_width):
    return (
        lax.broadcasted_iota(jnp.int32, shape, 0) // row_width
        == lax.broadcasted_iota(jnp.int32, shape, 1) // column_width
    ).astype(F32)


def dot32(left, right, contract=((1,), (0,))):
    return lax.dot_general(
        left, right, (contract, ((), ())), precision=HIGHEST, preferred_element_type=F32
    )


def attend_rows(sums, shift, spike, scale, heads):
    length = sums.shape[0]
    key_lanes, value_lanes = heads * HEAD_K, heads * HEAD_V

    def part(start, width):
        return sums[:, start : start + width]

    def rounded(array):
        return array.astype(BF16).astype(F32)

    query = rounded(part(0, key_lanes)) * HEAD_K ** (-0.5)
    keys = rounded(part(key_lanes, key_lanes))
    values = rounded(part(2 * key_lanes, value_lanes))
    decay_pre = part(2 * key_lanes + value_lanes, key_lanes) + shift
    gate = rounded(part(3 * key_lanes + value_lanes, value_lanes))
    log_sigmoid = jnp.minimum(decay_pre, 0.0) - jnp.log1p(jnp.exp(-jnp.abs(decay_pre)))
    c = log_sigmoid / switch_multiplier + spike
    row = lax.broadcasted_iota(jnp.int32, (length, key_lanes), 0)
    step = 1
    while step < length:
        c = c + jnp.where(row >= step, pltpu.roll(c, step, 0), 0.0)
        step *= 2

    spread = lanes_same((key_lanes, value_lanes), HEAD_K, HEAD_V)
    in_sub = lax.rem(row, SUB)
    out = dot32(query * keys, spread) * values
    for d in range(1, SUB):
        ok = in_sub >= d
        weight = jnp.exp(jnp.where(ok, c - pltpu.roll(c, d, 0), 0.0))
        product = jnp.where(ok, query * pltpu.roll(keys, d, 0) * weight, 0.0)
        out = out + dot32(product, spread) * pltpu.roll(values, d, 0)

    pieces = [jnp.zeros((SUB, value_lanes), F32)]
    stack = heads * SUB
    key_mask = lanes_same((stack, key_lanes), SUB, HEAD_K)
    value_mask = lanes_same((stack, value_lanes), SUB, HEAD_V)
    for start in range(SUB, length, SUB):
        edge = c[start - 1 : start]
        q_part = query[start : start + SUB] * jnp.exp(c[start : start + SUB] - edge)
        k_part = keys[:start] * jnp.exp(edge - c[:start])
        stacked = jnp.concatenate([q_part] * heads, axis=0) * key_mask
        scores = dot32(stacked, k_part, ((1,), (1,)))
        read = dot32(scores, values[:start]) * value_mask
        total = read[:SUB]
        for h in range(1, heads):
            total = total + read[h * SUB : (h + 1) * SUB]
        pieces.append(total)
    out = out + jnp.concatenate(pieces, axis=0)

    same = lanes_same((value_lanes, value_lanes), HEAD_V, HEAD_V)
    mean = dot32(out * out, same) / HEAD_V
    out = out * lax.rsqrt(mean + norm_eps) * scale
    return (out * (gate / (1.0 + jnp.exp(-gate)))).astype(BF16)


def causal_conv(content_tokens, taps, length):
    rows, columns = content_tokens.shape
    content_tokens = content_tokens.astype(F32).reshape(rows // length, length, columns)
    taps = taps.astype(F32)
    width = taps.shape[0]
    padded = jnp.pad(content_tokens, ((0, 0), (width - 1, 0), (0, 0)))
    total = jnp.zeros_like(content_tokens)
    for offset in range(width):
        total = total + padded[:, offset : offset + length] * taps[offset]
    return total.reshape(rows, columns)


def shards(
    sizes,
    incoming_features,
    attend_prenormal_scale,
    probe_matrix,
    lookup_matrix,
    content_matrix,
    forgetting_matrix,
    result_switch_matrix,
    forgetting_shift,
    spike_forget_logarithm,
    attend_unit_scale,
    attend_result_matrix,
    perceptron_scale,
    content_expand_matrix,
    switch_expand_matrix,
    content_kernel,
    switch_kernel,
    contract_matrix,
):
    n_rep, n_fs, n_tp = sizes
    rep = lax.axis_index("rep")
    length = incoming_features.shape[0]

    def mine(array, axis):
        size = array.shape[axis] // n_rep
        return lax.dynamic_slice_in_dim(array, rep * size, size, axis)

    project = jnp.concatenate(
        [
            mine(matrix, 1)
            for matrix in (
                probe_matrix,
                lookup_matrix,
                content_matrix,
                forgetting_matrix,
                result_switch_matrix,
            )
        ],
        axis=1,
    )
    spike_all = lax.all_to_all(
        spike_forget_logarithm, "rep", split_axis=1, concat_axis=0, tiled=True
    )
    expand = jnp.concatenate([mine(content_expand_matrix, 1), mine(switch_expand_matrix, 1)], axis=1)
    side = attend_result_matrix.shape[1]
    inside = side % 128 == 0
    outs = first_half(
        project,
        mine(attend_result_matrix, 0),
        expand,
        mine(contract_matrix, 0),
        incoming_features,
        attend_prenormal_scale,
        mine(forgetting_shift, 0),
        spike_all,
        mine(attend_unit_scale, 0),
        1 if inside else 0,
        inside,
        sizes,
    )
    if inside:
        expand_all, contract_all, middle, whole_mid = outs
    else:
        expand_all, contract_all, result_all, switched_result = outs
        result_all, contract_all = (
            array.reshape(n_fs, -1, side).swapaxes(0, 1).reshape(-1, n_fs * side)
            for array in (result_all, contract_all)
        )
        mixer_partial = jnp.dot(switched_result, result_all, preferred_element_type=F32)
        middle, whole_mid = reduce_group(
            mixer_partial.astype(BF16), incoming_features, sizes, True, 2
        )
    normed_mid = row_norm(whole_mid, perceptron_scale)
    both = jnp.dot(normed_mid, expand_all, preferred_element_type=F32).astype(BF16)
    half = both.shape[1] // 2
    conv_value = causal_conv(both[:, :half], mine(content_kernel, 1), length)
    conv_gated = causal_conv(both[:, half:], mine(switch_kernel, 1), length)
    hidden = (conv_value * jax.nn.gelu(conv_gated, approximate=True)).astype(BF16)
    down_partial = jnp.dot(hidden, contract_all, preferred_element_type=F32).astype(BF16)
    return reduce_group(down_partial, middle, sizes, False, 3)[0]


def solution(mesh):
    sizes = (mesh.shape["rep"], mesh.shape["fs"], mesh.shape["tp"])
    placed = (
        P(("rep", "fs"), "tp"),
        P(),
        P("fs", "tp"),
        P("fs", "tp"),
        P("fs", "tp"),
        P("fs", "tp"),
        P("fs", "tp"),
        P("tp"),
        P(("rep", "fs"), "tp"),
        P("tp"),
        P("tp", "fs"),
        P(),
        P("fs", "tp"),
        P("fs", "tp"),
        P(None, "tp"),
        P(None, "tp"),
        P("tp", "fs"),
    )
    return jax.shard_map(
        functools.partial(shards, sizes),
        mesh=mesh,
        in_specs=placed,
        out_specs=P(("rep", "fs"), "tp"),
        check_vma=False,
    )
```

time: 374 us -> 272 us (0.73)
  Pallas kernels: 331 us -> 240 us
  matrix products: 17.5 us -> 9.84 us
    pallas_call x3 -> x1, Pallas kernels: 285 us -> 224 us  [first_half(): pl.pallas_call(kernel, out_shape=out_shape, in_specs=[vmem] * 9, out_spec...]
    pallas_call x2 -> x1, Pallas kernels: 45.3 us -> 16.4 us  [reduce_group(): pl.pallas_call(kernel, out_shape=out_shape, in_specs=[vmem, vmem], out_sp...]
    dot_general x2 -> x0, matrix products: 7.69 us -> none  [the longest x1 5 us: shards(): sums = jnp.dot(normed, project_all, preferred_element_type=F32)]
    unnamed x35 -> x37, local copies, waits for them, and re-layouts: 8.66 us -> 3.75 us
  transfers between devices with their start and end apart: 1 -> 1, of which waited for: 0 -> 0; matrix products, arithmetic and copies ran while one was open for 4% -> 3% of each run, Pallas kernels for 73% -> 0%
where the time goes in v2:
time: 272 us; the launch traced here: 270 us
  Pallas kernels  240 us (88%)
  local copies, waits for them, and re-layouts  10.4 us (4%)
  matrix products  9.84 us (4%)
  other arithmetic  6.14 us (2%)
  starting transfers between devices  3.43 us (1%)
    pallas_call x1, Pallas kernels, first_half(): pl.pallas_call(kernel, out_shape=out_shape, in_specs=[vmem] * 9, out_spec...  224 us
    pallas_call x1, Pallas kernels, reduce_group(): pl.pallas_call(kernel, out_shape=out_shape, in_specs=[vmem, vmem], out_sp...  16.4 us
    dot_general x1, matrix products, shards(): jnp.dot(normed_mid, expand_all, preferred_element_type=F32).astype(BF16)  6.84 us
  transfers between devices with their start and end apart: 1, of which 0 were waited for; matrix products, arithmetic and copies ran while one was open for 3% of the time, Pallas kernels for 0%

profile of v2, /device:TPU:24, one launch (start us, length us, event | category | flops | bytes accessed | tf_op | source)
XLA Modules:
  0.0 270.2 jit_solution(2432211896326824425)
XLA Ops:
  0.0 0.0 copy-start
  0.0 0.0 copy-start.8
  0.0 0.0 copy-start.9
  0.0 0.0 copy-start.13
  0.0 0.0 copy-start.7
  0.1 0.0 copy-start.10
  0.1 0.0 copy-start.4
  0.1 1.8 copy_bitcast_fusion
  1.8 3.4 %all-to-all-start = ((f32[192,2,128]{2,0,1:T(8,128)}), f32[192,2,128]{2,0,1:T(8,128)S(1)}, u32[]{:S(2)}, u32[]{:S(2)}) async-start(f32[192,2,128]{2,0,1:T(8,128)} %copy_bitcast_fusion), calls=%async_computation | async-start | bytes 393216 | tf_op jit(solution)/shard_map/all_to_all | solution.py:542
  5.3 1.3 reshape.47.refs_5_
  6.6 0.7 convert_element_type.31
  7.3 0.0 copy-done
  7.3 0.9 constant_dynamic-slice_fusion.refs_3_
  8.1 0.0 copy-done.12
  8.1 0.0 copy-done.11
  8.2 0.0 copy-done.8
  8.2 0.0 copy-done.9
  8.3 0.0 copy-done.13
  8.3 0.7 dynamic-slice_convert_fusion.2
  8.9 0.0 copy-done.7
  8.9 0.0 copy-done.10
  9.0 0.0 copy-done.4
  9.0 1.1 constant_dynamic-slice_fusion.1
  10.1 0.0 copy-start.5
  10.2 0.0 copy-start.6
  10.2 0.0 copy-start.15
  10.2 1.1 pad_maximum_fusion.refs_2_
  11.2 0.0 copy-done.5
  11.2 0.7 dynamic-slice_dynamic-update-slice_fusion
  11.9 0.8 dynamic-slice_bitcast_fusion.refs_6_
  12.7 0.0 all-to-all-done
  12.7 0.0 copy-done.3
  12.7 0.7 copy-done.2
  13.4 223.8 %first_half.1 = (bf16[2048,2048]{1,0:T(8,128)(2,1)}, bf16[1024,2048]{1,0:T(8,128)(2,1)}, bf16[192,1024]{1,0:T(8,128)(2,1)}, bf16[384,2048]{1,0:T(8,128)(2,1)}) custom-call(bf16[256,896]{1,0:T(8,128)(2,1)} %copy-done.3, bf16[256,256]{1,0:T(8,128)(2,1)} %get-tuple-element.22.refs_1_, bf16[256,2048]{1,0:T(8,128)(2,1)} %pad_maximum_fusion.refs_2_, ...), custom_call_target="tpu_custom_call" | custom-call | tf_op jit(solution)/shard_map/first_half/pallas_call | solution.py:293
  237.1 0.0 copy-start.1
  237.1 1.9 fusion
  239.1 0.0 copy-done.1
  239.1 6.8 %convolution_convert_fusion = bf16[384,2048]{1,0:T(8,128)(2,1)S(1)} fusion(bf16[2048,2048]{1,0:T(8,128)(2,1)} %get-tuple-element.10, bf16[384,2048]{1,0:T(8,128)(2,1)S(1)} %copy-done.1, f32[2048]{0:T(1024)S(1)} %convert_element_type.31, f32[384]{0:T(512)S(1)} %add_rsqrt_fusion), kind=kOutput, calls=%fused_computation.5 | convolution fusion | flops 3225157632 | bytes 11544064 | tf_op jit(solution)/shard_map/dot_general | solution.py:575
  245.9 0.1 fusion.23
  246.1 0.2 convert.3
  246.2 0.2 convert.4
  246.4 0.5 fusion.5
  246.9 0.5 fusion.9
  247.3 0.5 fusion.19
  247.9 1.2 copy-done.14
  249.1 3.0 %convolution_convert_fusion.1.refs_0_ = bf16[384,2048]{1,0:T(8,128)(2,1)} fusion(bf16[384,1024]{1,0:T(8,128)(2,1)S(1)} %fusion.19, bf16[1024,2048]{1,0:T(8,128)(2,1)S(1)} %copy-done.14), kind=kOutput, calls=%fused_computation.6 | convolution fusion | flops 1611399168 | bytes 6553600 | tf_op jit(solution)/shard_map/dot_general | solution.py:580
  252.1 16.4 %reduce_group.1 = bf16[192,1024]{1,0:T(8,128)(2,1)} custom-call(bf16[384,2048]{1,0:T(8,128)(2,1)} %convolution_convert_fusion.1.refs_0_, bf16[192,1024]{1,0:T(8,128)(2,1)} %get-tuple-element.12.refs_1_), custom_call_target="tpu_custom_call" | custom-call | tf_op jit(solution)/shard_map/reduce_group/pallas_call | solution.py:402
  268.5 1.8 copy.26
  (15 shorter events, 0.1 us)
Async XLA Ops:
  0.0 7.3 %copy-start = (bf16[2048,256]{1,0:T(8,128)(2,1)S(1)}, bf16[2048,256]{1,0:T(8,128)(2,1)}, u32[]{:S(2)}) copy-start(bf16[2048,256]{1,0:T(8,128)(2,1)} %param.33) | copy-start | bytes 3145732
  0.0 8.1 %copy-start.12 = (bf16[3,2048]{1,0:T(4,128)(2,1)S(1)}, bf16[3,2048]{1,0:T(4,128)(2,1)}, u32[]{:S(2)}) copy-start(bf16[3,2048]{1,0:T(4,128)(2,1)} %param.31) | copy-start | bytes 36868
  0.0 8.1 %copy-start.11 = (bf16[3,2048]{1,0:T(4,128)(2,1)S(1)}, bf16[3,2048]{1,0:T(4,128)(2,1)}, u32[]{:S(2)}) copy-start(bf16[3,2048]{1,0:T(4,128)(2,1)} %param.32) | copy-start | bytes 36868
  0.0 8.2 %copy-start.8 = (bf16[256,256]{1,0:T(8,128)(2,1)S(1)}, bf16[256,256]{1,0:T(8,128)(2,1)}, u32[]{:S(2)}) copy-start(bf16[256,256]{1,0:T(8,128)(2,1)} %param.19) | copy-start | bytes 393220
  0.0 8.2 %copy-start.9 = (bf16[256,256]{1,0:T(8,128)(2,1)S(1)}, bf16[256,256]{1,0:T(8,128)(2,1)}, u32[]{:S(2)}) copy-start(bf16[256,256]{1,0:T(8,128)(2,1)} %param.20) | copy-start | bytes 393220
  0.0 8.2 %copy-start.13 = (bf16[512]{0:T(512)(128)(2,1)S(1)}, bf16[512]{0:T(512)(128)(2,1)}, u32[]{:S(2)}) copy-start(bf16[512]{0:T(512)(128)(2,1)} %param.26) | copy-start | bytes 3076
  0.0 8.9 %copy-start.7 = (bf16[256,512]{1,0:T(8,128)(2,1)S(1)}, bf16[256,512]{1,0:T(8,128)(2,1)}, u32[]{:S(2)}) copy-start(bf16[256,512]{1,0:T(8,128)(2,1)} %param.21) | copy-start | bytes 786436
  0.1 8.9 %copy-start.10 = (bf16[256,256]{1,0:T(8,128)(2,1)S(1)}, bf16[256,256]{1,0:T(8,128)(2,1)}, u32[]{:S(2)}) copy-start(bf16[256,256]{1,0:T(8,128)(2,1)} %param.22) | copy-start | bytes 393220
  0.1 8.9 %copy-start.4 = (bf16[256,2048]{1,0:T(8,128)(2,1)S(1)}, bf16[256,2048]{1,0:T(8,128)(2,1)}, u32[]{:S(2)}) copy-start(bf16[256,2048]{1,0:T(8,128)(2,1)} %param.30) | copy-start | bytes 3145732
  1.8 10.8 %all-to-all-start = ((f32[192,2,128]{2,0,1:T(8,128)}), f32[192,2,128]{2,0,1:T(8,128)S(1)}, u32[]{:S(2)}, u32[]{:S(2)}) async-start(f32[192,2,128]{2,0,1:T(8,128)} %copy_bitcast_fusion), calls=%async_computation | async-start | bytes 393216 | tf_op jit(solution)/shard_map/all_to_all | solution.py:542
  10.1 1.1 copy-start.5
  10.2 1.1 copy-start.6
  10.2 1.7 copy-start.15
  11.9 0.8 copy-start.3
  12.7 0.7 copy-start.2
  237.1 1.9 copy-start.1
  246.9 2.2 copy-start.14

commit v3 on v2

--- a/solution.py
+++ b/solution.py
@@ -125,15 +125,85 @@
                 return outs[w].at[pl.ds(offset + start, size), :]
             return outs[w].at[pl.ds(start, size), pl.ds(offset, across)]
 
-        far_copies, near_copies, own_copies = {}, {}, {}
+        near_copies, own_copies = {}, {}
+
+        def hop(c, step, way):
+            w, start, size = chunks[c]
+            spot = block(w, start, size, (a - way * step) * inner + b)
+            source = sources[w].at[pl.ds(start, size), :] if step == 0 else spot
+            at = step if way > 0 else outer - 1 + step
+            return pltpu.make_async_remote_copy(
+                src_ref=source,
+                dst_ref=spot,
+                send_sem=far_send.at[c, at],
+                recv_sem=far_recv.at[c, at],
+                device_id={"fs": (a + way) * inner + b},
+                device_id_type=MESH,
+            )
+
+        def turn(c, step, way, e):
+            w, start, size = chunks[c]
+            spot = block(w, start, size, (a - way * step) * inner + b)
+            at = step if way > 0 else outer - 1 + step
+            return pltpu.make_async_remote_copy(
+                src_ref=spot,
+                dst_ref=spot,
+                send_sem=near_send.at[c, at, e],
+                recv_sem=near_recv.at[c, at, e],
+                device_id={"fs": near[e]},
+                device_id_type=MESH,
+            )
+
+        def has(step, way):
+            return a >= step if way > 0 else a + step < outer
+
+        def goes(way):
+            return a + 1 < outer if way > 0 else a >= 1
 
         def launch_far(c):
-            w, start, size = chunks[c]
-            source, target = sources[w].at[pl.ds(start, size), :], block(w, start, size, fs)
-            far_copies[c] = [
-                send_to(source, target, far_send.at[c, d], far_recv.at[c, d], {"fs": index})
-                for d, index in enumerate(far)
-            ]
+            for way in (1, -1):
+
+                @pl.when(goes(way))
+                def _(way=way):
+                    hop(c, 0, way).start()
+
+        def forward(c):
+            for step in range(1, outer):
+                for way in (1, -1):
+
+                    @pl.when(has(step, way))
+                    def _(step=step, way=way):
+                        hop_in = hop(c, step - 1, way)
+                        hop_in.wait_recv()
+                        if step + 1 < outer:
+
+                            @pl.when(goes(way))
+                            def _():
+                                hop(c, step, way).start()
+
+                        for e in range(len(near)):
+                            turn(c, step, way, e).start()
+
+        def sent(c):
+            for way in (1, -1):
+
+                @pl.when(goes(way))
+                def _(way=way):
+                    hop(c, 0, way).wait_send()
+
+            for step in range(1, outer):
+                for way in (1, -1):
+
+                    @pl.when(has(step, way))
+                    def _(step=step, way=way):
+                        if step + 1 < outer:
+
+                            @pl.when(goes(way))
+                            def _():
+                                hop(c, step, way).wait_send()
+
+                        for e in range(len(near)):
+                            turn(c, step, way, e).wait_send()
 
         def launch_near(c):
             w, start, size = chunks[c]
@@ -147,26 +217,18 @@
             own_copies[c] = pltpu.make_async_copy(source, target, own_sem.at[c])
             own_copies[c].start()
 
-        def forward(c):
-            w, start, size = chunks[c]
-            for d in range(1, outer):
-                far_copies[c][d - 1].wait_recv()
-                held_block = block(w, start, size, lax.rem(a + outer - d, outer) * inner + b)
-                near_copies[c] += [
-                    send_to(
-                        held_block,
-                        held_block,
-                        near_send.at[c, d, e],
-                        near_recv.at[c, d, e],
-                        {"fs": index},
-                    )
-                    for e, index in enumerate(near)
-                ]
-
         def arrived(c):
             for copy in near_copies[c]:
                 copy.wait_recv()
             own_copies[c].wait()
+            for step in range(1, outer):
+                for way in (1, -1):
+
+                    @pl.when(has(step, way))
+                    def _(step=step, way=way):
+                        for e in range(len(near)):
+                            turn(c, step, way, e).wait_recv()
+
 
         first = [c for c in range(count) if chunks[c][0] == 0]
         second = [c for c in range(count) if chunks[c][0] == 1]
@@ -248,8 +310,9 @@
         for c in later:
             arrived(c)
         for c in range(count):
-            for copy in far_copies[c] + near_copies[c]:
+            for copy in near_copies[c]:
                 copy.wait_send()
+            sent(c)
 
     dma = pltpu.SemaphoreType.DMA
     vmem = pl.BlockSpec(memory_space=pltpu.VMEM)
@@ -280,10 +343,10 @@
     scratch += [
         pltpu.VMEM(full[0], BF16),
         pltpu.VMEM((rows, columns * n_tp), BF16),
-        dma((count, max(outer - 1, 1))),
-        dma((count, max(outer - 1, 1))),
-        dma((count, outer, max(inner - 1, 1))),
-        dma((count, outer, max(inner - 1, 1))),
+        dma((count, 2 * outer)),
+        dma((count, 2 * outer)),
+        dma((count, 2 * outer, max(inner - 1, 1))),
+        dma((count, 2 * outer, max(inner - 1, 1))),
         dma((count + 1,)),
         dma((group,)),
         dma((group,)),

time: 272 us -> 285 us (1.048)
  Pallas kernels: 240 us -> 250 us
    pallas_call x1, Pallas kernels: 224 us -> 234 us  [first_half(): pl.pallas_call(kernel, out_shape=out_shape, in_specs=[vmem] * 9, out_spec...]
where the time goes in v3:
time: 285 us; the launch traced here: 280 us
  Pallas kernels  250 us (88%)
  local copies, waits for them, and re-layouts  10.4 us (4%)
  matrix products  9.84 us (3%)
  other arithmetic  6.14 us (2%)
  starting transfers between devices  3.43 us (1%)
    pallas_call x1, Pallas kernels, first_half(): pl.pallas_call(kernel, out_shape=out_shape, in_specs=[vmem] * 9, out_spec...  234 us
    pallas_call x1, Pallas kernels, reduce_group(): pl.pallas_call(kernel, out_shape=out_shape, in_specs=[vmem, vmem], out_sp...  16.3 us
    dot_general x1, matrix products, shards(): jnp.dot(normed_mid, expand_all, preferred_element_type=F32).astype(BF16)  6.84 us
  transfers between devices with their start and end apart: 1, of which 0 were waited for; matrix products, arithmetic and copies ran while one was open for 3% of the time, Pallas kernels for 0%

profile of v3, /device:TPU:24, one launch (start us, length us, event | category | flops | bytes accessed | tf_op | source)
XLA Modules:
  0.0 280.5 jit_solution(3338905907047843366)
XLA Ops:
  0.0 0.0 copy-start
  0.0 0.0 copy-start.8
  0.0 0.0 copy-start.9
  0.0 0.0 copy-start.13
  0.0 0.0 copy-start.7
  0.1 0.0 copy-start.10
  0.1 0.0 copy-start.4
  0.1 1.8 copy_bitcast_fusion
  1.8 3.4 %all-to-all-start = ((f32[192,2,128]{2,0,1:T(8,128)}), f32[192,2,128]{2,0,1:T(8,128)S(1)}, u32[]{:S(2)}, u32[]{:S(2)}) async-start(f32[192,2,128]{2,0,1:T(8,128)} %copy_bitcast_fusion), calls=%async_computation | async-start | bytes 393216 | tf_op jit(solution)/shard_map/all_to_all | solution.py:605
  5.3 1.3 reshape.47.refs_5_
  6.6 0.7 convert_element_type.31
  7.3 0.0 copy-done
  7.3 0.9 constant_dynamic-slice_fusion.refs_3_
  8.1 0.0 copy-done.12
  8.1 0.0 copy-done.11
  8.2 0.0 copy-done.8
  8.2 0.0 copy-done.9
  8.3 0.0 copy-done.13
  8.3 0.7 dynamic-slice_convert_fusion.2
  8.9 0.0 copy-done.7
  8.9 0.0 copy-done.10
  9.0 0.0 copy-done.4
  9.0 1.1 constant_dynamic-slice_fusion.1
  10.1 0.0 copy-start.5
  10.2 0.0 copy-start.6
  10.2 0.0 copy-start.15
  10.2 1.1 pad_maximum_fusion.refs_2_
  11.2 0.0 copy-done.5
  11.2 0.0 copy-done.6
  11.2 0.7 dynamic-slice_dynamic-update-slice_fusion
  11.9 0.8 dynamic-slice_bitcast_fusion.refs_6_
  12.7 0.0 all-to-all-done
  12.7 0.0 copy-done.3
  12.7 0.7 copy-done.2
  13.4 234.1 %first_half.1 = (bf16[2048,2048]{1,0:T(8,128)(2,1)}, bf16[1024,2048]{1,0:T(8,128)(2,1)}, bf16[192,1024]{1,0:T(8,128)(2,1)}, bf16[384,2048]{1,0:T(8,128)(2,1)}) custom-call(bf16[256,896]{1,0:T(8,128)(2,1)} %copy-done.3, bf16[256,256]{1,0:T(8,128)(2,1)} %get-tuple-element.22.refs_1_, bf16[256,2048]{1,0:T(8,128)(2,1)} %pad_maximum_fusion.refs_2_, ...), custom_call_target="tpu_custom_call" | custom-call | tf_op jit(solution)/shard_map/first_half/pallas_call | solution.py:356
  247.5 1.9 fusion
  249.4 6.8 %convolution_convert_fusion = bf16[384,2048]{1,0:T(8,128)(2,1)S(1)} fusion(bf16[2048,2048]{1,0:T(8,128)(2,1)} %get-tuple-element.10, bf16[384,2048]{1,0:T(8,128)(2,1)S(1)} %copy-done.1, f32[2048]{0:T(1024)S(1)} %convert_element_type.31, f32[384]{0:T(512)S(1)} %add_rsqrt_fusion), kind=kOutput, calls=%fused_computation.5 | convolution fusion | flops 3225157632 | bytes 11544064 | tf_op jit(solution)/shard_map/dot_general | solution.py:638
  256.2 0.1 fusion.23
  256.4 0.2 convert.3
  256.5 0.2 convert.4
  256.7 0.5 fusion.5
  257.2 0.0 copy-start.14
  257.2 0.5 fusion.9
  257.7 0.5 fusion.19
  258.2 1.2 copy-done.14
  259.4 3.0 %convolution_convert_fusion.1.refs_0_ = bf16[384,2048]{1,0:T(8,128)(2,1)} fusion(bf16[384,1024]{1,0:T(8,128)(2,1)S(1)} %fusion.19, bf16[1024,2048]{1,0:T(8,128)(2,1)S(1)} %copy-done.14), kind=kOutput, calls=%fused_computation.6 | convolution fusion | flops 1611399168 | bytes 6553600 | tf_op jit(solution)/shard_map/dot_general | solution.py:643
  262.4 16.3 %reduce_group.1 = bf16[192,1024]{1,0:T(8,128)(2,1)} custom-call(bf16[384,2048]{1,0:T(8,128)(2,1)} %convolution_convert_fusion.1.refs_0_, bf16[192,1024]{1,0:T(8,128)(2,1)} %get-tuple-element.12.refs_1_), custom_call_target="tpu_custom_call" | custom-call | tf_op jit(solution)/shard_map/reduce_group/pallas_call | solution.py:465
  278.7 1.8 copy.26
  (15 shorter events, 0.1 us)
Async XLA Ops:
  0.0 7.3 %copy-start = (bf16[2048,256]{1,0:T(8,128)(2,1)S(1)}, bf16[2048,256]{1,0:T(8,128)(2,1)}, u32[]{:S(2)}) copy-start(bf16[2048,256]{1,0:T(8,128)(2,1)} %param.33) | copy-start | bytes 3145732
  0.0 8.1 %copy-start.12 = (bf16[3,2048]{1,0:T(4,128)(2,1)S(1)}, bf16[3,2048]{1,0:T(4,128)(2,1)}, u32[]{:S(2)}) copy-start(bf16[3,2048]{1,0:T(4,128)(2,1)} %param.31) | copy-start | bytes 36868
  0.0 8.1 %copy-start.11 = (bf16[3,2048]{1,0:T(4,128)(2,1)S(1)}, bf16[3,2048]{1,0:T(4,128)(2,1)}, u32[]{:S(2)}) copy-start(bf16[3,2048]{1,0:T(4,128)(2,1)} %param.32) | copy-start | bytes 36868
  0.0 8.2 %copy-start.8 = (bf16[256,256]{1,0:T(8,128)(2,1)S(1)}, bf16[256,256]{1,0:T(8,128)(2,1)}, u32[]{:S(2)}) copy-start(bf16[256,256]{1,0:T(8,128)(2,1)} %param.19) | copy-start | bytes 393220
  0.0 8.2 %copy-start.9 = (bf16[256,256]{1,0:T(8,128)(2,1)S(1)}, bf16[256,256]{1,0:T(8,128)(2,1)}, u32[]{:S(2)}) copy-start(bf16[256,256]{1,0:T(8,128)(2,1)} %param.20) | copy-start | bytes 393220
  0.0 8.2 %copy-start.13 = (bf16[512]{0:T(512)(128)(2,1)S(1)}, bf16[512]{0:T(512)(128)(2,1)}, u32[]{:S(2)}) copy-start(bf16[512]{0:T(512)(128)(2,1)} %param.26) | copy-start | bytes 3076
  0.0 8.9 %copy-start.7 = (bf16[256,512]{1,0:T(8,128)(2,1)S(1)}, bf16[256,512]{1,0:T(8,128)(2,1)}, u32[]{:S(2)}) copy-start(bf16[256,512]{1,0:T(8,128)(2,1)} %param.21) | copy-start | bytes 786436
  0.1 8.9 %copy-start.10 = (bf16[256,256]{1,0:T(8,128)(2,1)S(1)}, bf16[256,256]{1,0:T(8,128)(2,1)}, u32[]{:S(2)}) copy-start(bf16[256,256]{1,0:T(8,128)(2,1)} %param.22) | copy-start | bytes 393220
  0.1 8.9 %copy-start.4 = (bf16[256,2048]{1,0:T(8,128)(2,1)S(1)}, bf16[256,2048]{1,0:T(8,128)(2,1)}, u32[]{:S(2)}) copy-start(bf16[256,2048]{1,0:T(8,128)(2,1)} %param.30) | copy-start | bytes 3145732
  1.8 10.8 %all-to-all-start = ((f32[192,2,128]{2,0,1:T(8,128)}), f32[192,2,128]{2,0,1:T(8,128)S(1)}, u32[]{:S(2)}, u32[]{:S(2)}) async-start(f32[192,2,128]{2,0,1:T(8,128)} %copy_bitcast_fusion), calls=%async_computation | async-start | bytes 393216 | tf_op jit(solution)/shard_map/all_to_all | solution.py:605
  10.1 1.1 copy-start.5
  10.2 1.1 copy-start.6
  10.2 1.7 copy-start.15
  11.9 0.8 copy-start.3
  12.7 0.7 copy-start.2
  247.5 1.9 copy-start.1
  257.2 2.2 copy-start.14
